TPU v7x, 256 devices: a whole 4x4x8 slice. The times are simulated.
256 devices in a mesh: ep: 64 (over z, x, core), tp: 4 (over y).
Axes of the slice: x: 4, y: 4, z: 8, core: 2. Of those that a mesh axis runs over, the one named last changes fastest.
Arguments:
- query_latent: bfloat16 [16384, 512], P(('ep', 'tp')), may hold values from -6 to 6
- key_latent: bfloat16 [16384, 256], P(('ep', 'tp')), may hold values from -6 to 6
- rotary_key: bfloat16 [16384, 32], P(('ep', 'tp')), may hold values from -140 to 140
- query_gain: float32 [512], replicated, may hold values from 0.1 to 1.9
- latent_gain: float32 [256], replicated, may hold values from 0.1 to 1.9
- query_content: bfloat16 [512, 512], replicated, may hold values from -0.625 to 0.625
- query_rotary: bfloat16 [512, 256], replicated, may hold values from -0.625 to 0.625
- key_content: bfloat16 [256, 512], replicated, may hold values from -0.375 to 0.375
- value_weight: bfloat16 [256, 512], replicated, may hold values from -0.375 to 0.375
- output_weight: bfloat16 [512, 2048], P('tp'), may hold values from -1 to 1
- expert_input: bfloat16 [16384, 2048], P(('ep', 'tp')), may hold values from -6 to 6
- norm_gain: float32 [2048], replicated, may hold values from 0.1 to 1.9
- routes: int32 [16384, 2], P(('ep', 'tp')), may hold values from 0 to 127, all different within a row; in each aligned block of 64 rows (0 to 63, 64 to 127, ...) at most 2 rows name the same one
- route_weight: float32 [16384, 2], P(('ep', 'tp')), may hold values from 0.25 to 2
- expert_gate: bfloat16 [128, 2048, 1024], P('ep', None, 'tp'), may hold values from -0.125 to 0.125
- expert_up: bfloat16 [128, 2048, 1024], P('ep', None, 'tp'), may hold values from -0.125 to 0.125
- expert_down: bfloat16 [128, 1024, 2048], P('ep', 'tp'), may hold values from -0.1875 to 0.1875
- shared_gate: bfloat16 [2048, 1024], P(None, 'tp'), may hold values from -0.125 to 0.125
- shared_up: bfloat16 [2048, 1024], P(None, 'tp'), may hold values from -0.125 to 0.125
- shared_down: bfloat16 [1024, 2048], P('tp'), may hold values from -0.1875 to 0.1875
Outputs:
- mixer_out: bfloat16 [16384, 2048], P(('ep', 'tp'))
- expert_out: bfloat16 [16384, 2048], P(('ep', 'tp'))
Inputs may be any that keep to these rules, and one draw needn't show every extreme that they name: `routes`: each row names 2 different experts. Within the rows of one device (aligned blocks of 64 rows) no expert is named by more than 2 rows, and in every draw some expert is named by exactly 2 rows of some device.
All inputs are finite; a program needn't handle non-finite values.
Results may differ from a plain program's by a relative error of at most 0.013.
The roundings to bfloat16 on the way count: a program that leaves them out, or rounds other values in their place, can miss the bound.
Values may be sent and summed in bfloat16 or wider, within the bound.
A program may use at most 128 MiB of HBM per device.

v0:
```python
import math

import jax
import jax.numpy as jnp
from jax import lax
from jax.sharding import PartitionSpec as P

HEADS = 8
CONTENT = 64
ROTARY = 32
VALUE = 64


norm_eps = 1e-06
rope_base = 10000.0


def side_by_side(arrays, axis, dim, along):
    widths = [math.prod(a.shape[along:]) for a in arrays]
    both = jnp.concatenate(
        [a.reshape(*a.shape[:along], w) for a, w in zip(arrays, widths)], axis=along
    )
    out = lax.all_gather(both, axis, axis=dim, tiled=True)
    tiles = jnp.split(out, [sum(widths[:k]) for k in range(1, len(widths))], axis=along)
    return tuple((b.reshape(*out.shape[:along], *a.shape[along:]) for a, b in zip(arrays, tiles)))


def sent_together(arrays, axis, dim, along):
    ends, at = ([], 0)
    for a in arrays[:-1]:
        at += a.shape[along]
        ends.append(at)
    both = jnp.concatenate(arrays, axis=along)
    return tuple(jnp.split(lax.all_gather(both, axis, axis=dim, tiled=True), ends, axis=along))


def cut_along(array, dim, peers):
    before, after = (array.shape[:dim], array.shape[dim + 1 :])
    return jnp.moveaxis(array.reshape(*before, peers, -1, *after), dim, 0)


def sum_at_owner(array, axis, dim):
    tiles = cut_along(array, dim, lax.axis_size(axis))
    arrived = lax.all_to_all(tiles, axis, split_axis=0, concat_axis=0, tiled=True)
    return arrived.astype(jnp.float32).sum(axis=0)


def rms_rows(entries, gain_row):
    widened = entries.astype(jnp.float32)
    return widened * lax.rsqrt(jnp.mean(widened * widened, -1, keepdims=True) + norm_eps) * gain_row


def turn_pairs(entries, positions):
    width_full = entries.shape[-1]
    frequency = rope_base ** (-jnp.arange(width_full // 2, dtype=jnp.float32) * 2.0 / width_full)
    angles = positions.astype(jnp.float32)[:, None] * frequency[None, :]
    cosine = jnp.cos(angles)[:, None, :]
    sine_part = jnp.sin(angles)[:, None, :]
    even_part = entries[..., 0::2]
    odd_part = entries[..., 1::2]
    joined = jnp.stack(
        [even_part * cosine - odd_part * sine_part, even_part * sine_part + odd_part * cosine], -1
    )
    return joined.reshape(entries.shape)


def absorb_block(carried, query_part, query_turn, key_part, key_turn, value_rows, score_scale):
    running_peak, running_total, summed = carried
    scores = jnp.einsum("qhc,khc->qhk", query_part, key_part, preferred_element_type=jnp.float32)
    scores = scores + jnp.einsum(
        "qhr,kr->qhk", query_turn, key_turn, preferred_element_type=jnp.float32
    )
    scores = scores * score_scale
    new_peak = jnp.maximum(running_peak, jnp.max(scores, -1))
    factor = jnp.exp(running_peak - new_peak)
    weights = jnp.exp(scores - new_peak[..., None])
    running_total = running_total * factor + jnp.sum(weights, -1)
    summed = summed * factor[..., None] + jnp.einsum(
        "qhk,khv->qhv", weights.astype(jnp.bfloat16), value_rows, preferred_element_type=jnp.float32
    )
    return (new_peak, running_total, summed)


def absorb_piece(carried, query_part, query_turn, key_part, key_turn, value_rows, score_scale):
    row_count = key_part.shape[0]
    key_block = math.gcd(row_count, 2048)
    block_count = row_count // key_block

    def advance(state, pieces):
        return (
            absorb_block(
                state, query_part, query_turn, pieces[0], pieces[1], pieces[2], score_scale
            ),
            None,
        )

    stacked = (
        key_part.reshape((block_count, key_block) + key_part.shape[1:]),
        key_turn.reshape(block_count, key_block, key_turn.shape[1]),
        value_rows.reshape((block_count, key_block) + value_rows.shape[1:]),
    )
    carried, ignored = lax.scan(advance, carried, stacked)
    return carried


def expand_keys(latent_rows, key_columns, value_columns, head_local):
    row_count = latent_rows.shape[0]
    key_part = (
        jnp.dot(latent_rows, key_columns, preferred_element_type=jnp.float32)
        .astype(jnp.bfloat16)
        .reshape(row_count, head_local, CONTENT)
    )
    value_rows = (
        jnp.dot(latent_rows, value_columns, preferred_element_type=jnp.float32)
        .astype(jnp.bfloat16)
        .reshape(row_count, head_local, VALUE)
    )
    return (key_part, value_rows)


def expert_terms(row_block, gate_weight, up_weight, down_weight):
    gated = jnp.einsum("secd,edf->secf", row_block, gate_weight, preferred_element_type=jnp.float32)
    lifted = jnp.einsum("secd,edf->secf", row_block, up_weight, preferred_element_type=jnp.float32)
    hidden = (jax.nn.silu(gated) * lifted).astype(jnp.bfloat16)
    return jnp.einsum("secf,efd->secd", hidden, down_weight, preferred_element_type=jnp.float32)


def shared_terms(row_block, gate_weight, up_weight, down_weight):
    gated = jnp.dot(row_block, gate_weight, preferred_element_type=jnp.float32)
    lifted = jnp.dot(row_block, up_weight, preferred_element_type=jnp.float32)
    hidden = (jax.nn.silu(gated) * lifted).astype(jnp.bfloat16)
    return jnp.dot(hidden, down_weight, preferred_element_type=jnp.float32)


def shards(
    query_latent,
    key_latent,
    rotary_key,
    query_gain,
    latent_gain,
    query_content,
    query_rotary,
    key_content,
    value_weight,
    output_weight,
    expert_input,
    norm_gain,
    routes,
    route_weight,
    expert_gate,
    expert_up,
    expert_down,
    shared_gate,
    shared_up,
    shared_down,
):
    group_size = lax.axis_size("tp")
    expert_groups = lax.axis_size("ep")
    own_rows = query_latent.shape[0]
    head_local = HEADS // group_size
    head_index = lax.axis_index("tp")
    group_rows_count = own_rows * group_size
    group_start = lax.axis_index("ep") * group_rows_count
    own_start = group_start + head_index * own_rows
    score_scale = (CONTENT + ROTARY) ** (-0.5)
    query_normed = rms_rows(query_latent, query_gain).astype(jnp.bfloat16)
    latent_normed = rms_rows(key_latent, latent_gain).astype(jnp.bfloat16)
    own_positions = own_start + jnp.arange(own_rows, dtype=jnp.int32)
    key_turned = turn_pairs(rotary_key.astype(jnp.float32)[:, None, :], own_positions)[
        :, 0, :
    ].astype(jnp.bfloat16)
    token_rows = expert_input.shape[0]
    picks = routes.shape[1]
    local_experts = expert_gate.shape[0]
    expert_total = local_experts * expert_groups
    capacity = 2 * token_rows * picks // expert_total
    slot_total = expert_total * capacity
    model_width = expert_input.shape[1]
    expert_normed = rms_rows(expert_input, norm_gain).astype(jnp.bfloat16)
    flat_routes = routes.reshape(-1)
    marks = (flat_routes[:, None] == jnp.arange(expert_total, dtype=jnp.int32)[None, :]).astype(
        jnp.int32
    )
    ranks = jnp.sum((jnp.cumsum(marks, 0) - marks) * marks, 1)
    targets = flat_routes * capacity + ranks
    picker = (jnp.arange(slot_total, dtype=jnp.int32)[:, None] == targets[None, :]).astype(
        jnp.int32
    )
    picker = jnp.sum(picker.reshape(slot_total, token_rows, picks), 2).astype(jnp.bfloat16)
    outgoing = jnp.dot(picker, expert_normed, preferred_element_type=jnp.float32).astype(
        jnp.bfloat16
    )
    outgoing = outgoing.reshape(expert_groups, local_experts, capacity, model_width)
    received = lax.all_to_all(outgoing, "ep", split_axis=0, concat_axis=0, tiled=True)
    group_query, group_latent, group_turn = (
        lax.all_gather(query_normed, "tp", axis=0, tiled=True),
        lax.all_gather(latent_normed, "tp", axis=0, tiled=True),
        lax.all_gather(key_turned, "tp", axis=0, tiled=True),
    )
    gathered_rows, gathered_tokens = side_by_side((received, expert_normed), "tp", 0, 1)
    positions = group_start + jnp.arange(group_rows_count, dtype=jnp.int32)
    content_columns = lax.dynamic_slice_in_dim(
        query_content, head_index * head_local * CONTENT, head_local * CONTENT, 1
    )
    rotary_columns = lax.dynamic_slice_in_dim(
        query_rotary, head_index * head_local * ROTARY, head_local * ROTARY, 1
    )
    query_part = (
        jnp.dot(group_query, content_columns, preferred_element_type=jnp.float32)
        .astype(jnp.bfloat16)
        .reshape(group_rows_count, head_local, CONTENT)
    )
    query_turn = turn_pairs(
        jnp.dot(group_query, rotary_columns, preferred_element_type=jnp.float32).reshape(
            group_rows_count, head_local, ROTARY
        ),
        positions,
    ).astype(jnp.bfloat16)
    key_columns = lax.dynamic_slice_in_dim(
        key_content, head_index * head_local * CONTENT, head_local * CONTENT, 1
    )
    value_columns = lax.dynamic_slice_in_dim(
        value_weight, head_index * head_local * VALUE, head_local * VALUE, 1
    )
    carry_start = (
        jnp.full((group_rows_count, head_local), -jnp.inf, jnp.float32),
        jnp.zeros((group_rows_count, head_local), jnp.float32),
        jnp.zeros((group_rows_count, head_local, VALUE), jnp.float32),
    )
    own_keys, own_values = expand_keys(group_latent, key_columns, value_columns, head_local)
    pieces = sent_together(
        (
            own_keys.reshape(group_rows_count, head_local * CONTENT),
            group_turn,
            own_values.reshape(group_rows_count, head_local * VALUE),
        ),
        "ep",
        0,
        1,
    )
    row_count = pieces[0].shape[0]
    running_peak, running_total, summed = absorb_piece(
        carry_start,
        query_part,
        query_turn,
        pieces[0].reshape(row_count, head_local, CONTENT),
        pieces[1],
        pieces[2].reshape(row_count, head_local, VALUE),
        score_scale,
    )
    attended = (
        (summed / running_total[..., None])
        .astype(jnp.bfloat16)
        .reshape(group_rows_count, head_local * VALUE)
    )
    routed_term = expert_terms(gathered_rows, expert_gate, expert_up, expert_down)
    shared_term = shared_terms(gathered_tokens, shared_gate, shared_up, shared_down)
    mixer_sum = sum_at_owner(
        jnp.dot(attended, output_weight, preferred_element_type=jnp.float32).astype(jnp.bfloat16),
        "tp",
        0,
    )
    routed_sum, shared_sum = (
        lax.psum_scatter(
            routed_term.astype(jnp.bfloat16), "tp", scatter_dimension=0, tiled=True
        ).astype(jnp.float32),
        lax.psum_scatter(
            shared_term.astype(jnp.bfloat16), "tp", scatter_dimension=0, tiled=True
        ).astype(jnp.float32),
    )
    mixer_out = mixer_sum.astype(jnp.bfloat16)
    returned = lax.all_to_all(
        routed_sum.astype(jnp.bfloat16), "ep", split_axis=0, concat_axis=0, tiled=True
    )
    returned = returned.reshape(slot_total, model_width)
    picked = jnp.take(returned, targets, axis=0).reshape(token_rows, picks, model_width)
    combined = jnp.sum(route_weight[..., None] * picked.astype(jnp.float32), 1) + shared_sum
    expert_out = combined.astype(jnp.bfloat16)
    return (mixer_out, expert_out)


def solution(mesh):
    in_specs = (
        P(("ep", "tp"), None),
        P(("ep", "tp"), None),
        P(("ep", "tp"), None),
        P(),
        P(),
        P(),
        P(),
        P(),
        P(),
        P("tp", None),
        P(("ep", "tp"), None),
        P(),
        P(("ep", "tp"), None),
        P(("ep", "tp"), None),
        P("ep", None, "tp"),
        P("ep", None, "tp"),
        P("ep", "tp", None),
        P(None, "tp"),
        P(None, "tp"),
        P("tp", None),
    )
    out_specs = (P(("ep", "tp"), None), P(("ep", "tp"), None))
    return jax.shard_map(shards, mesh=mesh, in_specs=in_specs, out_specs=out_specs, check_vma=False)
```

profile of v0, /device:TPU:1, one launch (start us, length us, event | category | flops | bytes accessed | tf_op | source)
XLA Modules:
  0.0 343.7 jit_solution(191552301445275806)
XLA Ops:
  13.9 41.4 %all_to_all.15 = bf16[64,2,2,2048]{3,2,1,0:T(2,128)(2,1)} all-to-all(bf16[64,2,2,2048]{3,2,1,0:T(2,128)(2,1)} %reshape.278), channel_id=1, replica_groups=mesh['ep'=64,'tp'=4] {'ep'}, dimensions={0} | all-to-all | bytes 2097152 | tf_op jit(solution)/shard_map/all_to_all | solution.py:194
  55.3 1.9 reshape.279
  58.6 9.6 %all-gather = bf16[4,64,32]{1,2,0:T(8,128)(2,1)S(1)} all-gather(bf16[1,64,32]{1,2,0:T(8,128)(2,1)S(1)} %bitcast.138), channel_id=1, replica_groups=mesh['ep'=64,'tp'=4] {'tp'}, dimensions={0}, use_global_device_ids=true | all-gather | bytes 20480 | tf_op jit(solution)/shard_map/all_gather | solution.py:198
  68.5 10.9 %all_gather.15 = bf16[256,256]{1,0:T(8,128)(2,1)S(1)} all-gather(bf16[64,256]{1,0:T(8,128)(2,1)S(1)} %fusion.66), channel_id=1, replica_groups=mesh['ep'=64,'tp'=4] {'tp'}, dimensions={0}, use_global_device_ids=true | all-gather | bytes 163840 | tf_op jit(solution)/shard_map/all_gather | solution.py:197
  82.6 12.3 %all_gather.18 = bf16[256,512]{1,0:T(8,128)(2,1)S(1)} all-gather(bf16[64,512]{1,0:T(8,128)(2,1)S(1)} %fusion.59), channel_id=1, replica_groups=mesh['ep'=64,'tp'=4] {'tp'}, dimensions={0}, use_global_device_ids=true | all-gather | bytes 327680 | tf_op jit(solution)/shard_map/all_gather | solution.py:196
  97.5 20.7 %all-gather.6.cloned.1.call-done = bf16[256,10240]{1,0:T(8,128)(2,1)} async-done(((bf16[64,10240]{1,0:T(8,128)(2,1)}), bf16[256,10240]{1,0:T(8,128)(2,1)}) %all-gather.6.cloned.1.call-update) | async-done | bytes 5242896 | tf_op jit(solution)/shard_map/all_gather | solution.py:23
  118.2 4.6 %split.23 = bf16[256,8192]{1,0:T(8,128)(2,1)} slice(bf16[256,10240]{1,0:T(8,128)(2,1)} %all-gather.6.cloned.1.call-done), slice={[0:256], [0:8192]} | slice | bytes 8388608 | tf_op jit(solution)/shard_map/split | solution.py:24
  122.8 6.4 %copy.95 = bf16[256,8192]{0,1:T(8,128)(2,1)} copy(bf16[256,8192]{1,0:T(8,128)(2,1)} %split.23) | data formatting | bytes 8388608
  129.2 5.6 %fusion.29 = f32[256,2,2,256]{3,0,2,1:T(8,128)} fusion(bf16[256,2,2,2048]{0,3,2,1:T(8,128)(2,1)} %bitcast.131, bf16[2,2048,256]{2,1,0:T(8,128)(2,1)} %param.36), kind=kOutput, calls=%fused_computation.35 | convolution fusion | flops 1073741824 | bytes 7340032 | tf_op jit(solution)/shard_map/secd,edf->secf/dot_general | solution.py:122
  134.8 7.5 %convert_bitcast_fusion = bf16[256,2,2,2048]{3,0,2,1:T(8,128)(2,1)} fusion(bf16[2,256,2048]{2,1,0:T(8,128)(2,1)S(1)} %copy-done, bf16[256,2,2,2048]{0,3,2,1:T(8,128)(2,1)} %bitcast.132, bf16[2,2048,256]{2,1,0:T(8,128)(2,1)} %param.37, f32[256,2,2,256]{3,0,2,1:T(8,128)} %fusion.29), kind=kOutput, calls=%fused_computation.26 | convolution fusion | flops 2151153664 | bytes 13631488 | tf_op jit(solution)/shard_map/secf,efd->secd/dot_general | solution.py:125
  142.4 66.4 %all-gather.4.cloned.1.call-done = bf16[16384,288]{0,1:T(8,128)(2,1)} async-done(((bf16[256,288]{0,1:T(8,128)(2,1)}), bf16[16384,288]{0,1:T(8,128)(2,1)}) %all-gather.4.cloned.1.call-update) | async-done | bytes 9437200 | tf_op jit(solution)/shard_map/all_gather | solution.py:34
  208.8 4.1 %fusion.93 = (bf16[16384,128]{0,1:T(8,128)(2,1)S(1)}, bf16[16384,128]{0,1:T(8,128)(2,1)S(1)}) fusion(bf16[16384,288]{0,1:T(8,128)(2,1)} %all-gather.4.cloned.1.call-done), kind=kLoop, calls=%fused_computation.129 | loop fusion | bytes 16777216 | tf_op jit(solution)/shard_map/split | solution.py:34
  212.9 3.2 copy.98
  216.1 4.3 %copy.79 = bf16[8,2048,2,64]{1,3,2,0:T(8,128)(2,1)} copy(bf16[8,2048,2,64]{1,0,3,2:T(8,128)(2,1)S(1)} %bitcast.126) | data formatting | bytes 8388608
  220.4 3.2 copy.97
  223.6 4.3 %copy.77 = bf16[8,2048,2,64]{1,3,2,0:T(8,128)(2,1)} copy(bf16[8,2048,2,64]{1,0,3,2:T(8,128)(2,1)S(1)} %bitcast.127) | data formatting | bytes 8388608
  228.0 40.6 %while.15 = (s32[]{:T(128)}, f32[256,2]{0,1:T(2,128)S(1)}, f32[256,2]{0,1:T(2,128)S(1)}, f32[256,2,64]{0,2,1:T(8,128)S(1)}, bf16[8,2048,2,64]{1,3,2,0:T(8,128)(2...) while((s32[]{:T(128)}, f32[256,2]{0,1:T(2,128)S(1)}, ...), condition=%wide.region_5.6_spmd.clone, body=%wide.region_2.5_spmd.clone.sunk | while | flops 342985216 | bytes 22544524 | solution.py:102
  231.4 1.8 fusion.129
  236.5 1.8 fusion.129
  246.6 1.9 fusion.129
  251.7 1.9 fusion.129
  256.7 1.8 fusion.129
  261.8 1.8 fusion.129
  266.8 1.8 fusion.129
  270.2 4.1 %all-to-all-start = ((bf16[4,64,2048]{2,1,0:T(8,128)(2,1)}), bf16[4,64,2048]{2,1,0:T(8,128)(2,1)S(1)}, u32[]{:S(2)}, u32[]{:S(2)}) async-start(bf16[4,64,2048]{2,1,0:T(8,128)(2,1)} %bitcast.10), calls=%async_computation | async-start | bytes 2097152 | tf_op jit(solution)/shard_map/all_to_all | solution.py:44
  274.3 2.0 fusion.44
  276.3 3.3 copy.87
  279.6 9.3 %all-to-all-done = bf16[4,64,2048]{2,1,0:T(8,128)(2,1)S(1)} async-done(((bf16[4,64,2048]{2,1,0:T(8,128)(2,1)}), bf16[4,64,2048]{2,1,0:T(8,128)(2,1)S(1)}, u32[]{:S(2)}, u32[]{:S(2)}) %all-to-all-start) | async-done | bytes 1048608 | tf_op jit(solution)/shard_map/all_to_all | solution.py:44
  289.0 11.1 %all-to-all-start.2 = ((bf16[64,2,2,2048]{3,2,1,0:T(2,128)(2,1)}), bf16[64,2,2,2048]{3,2,1,0:T(2,128)(2,1)}, u32[]{:S(2)}, u32[]{:S(2)}) async-start(bf16[64,2,2,2048]{3,2,1,0:T(2,128)(2,1)} %copy.87), calls=%async_computation.3 | async-start | bytes 2097152 | tf_op jit(solution)/shard_map/all_to_all | solution.py:272
  300.1 3.9 %convolution_convert_fusion.1 = bf16[256,2048]{1,0:T(8,128)(2,1)} fusion(bf16[256,2048]{1,0:T(8,128)(2,1)S(1)} %copy-done.10, bf16[2048,256]{1,0:T(8,128)(2,1)} %param.40, bf16[256,10240]{1,0:T(8,128)(2,1)} %all-gather.6.cloned.1.call-done, f32[256,256]{1,0:T(8,128)S(1)} %fusion.44), kind=kOutput, calls=%fused_computation.28 | convolution fusion | flops 537788416 | bytes 4456448 | tf_op jit(solution)/shard_map/dot_general | solution.py:132
  305.4 22.7 %all-to-all-done.2 = bf16[64,2,2,2048]{3,2,1,0:T(2,128)(2,1)} async-done(((bf16[64,2,2,2048]{3,2,1,0:T(2,128)(2,1)}), bf16[64,2,2,2048]{3,2,1,0:T(2,128)(2,1)}, u32[]{:S(2)}, u32[]{:S(2)}) %all-to-all-start.2) | async-done | bytes 1048608 | tf_op jit(solution)/shard_map/all_to_all | solution.py:272
  332.9 2.5 multiply_reduce_fusion
  (145 shorter events, 50.6 us)
Async XLA Ops:
  7.2 127.6 %copy-start = (bf16[2,256,2048]{2,1,0:T(8,128)(2,1)S(1)}, bf16[2,256,2048]{2,1,0:T(8,128)(2,1)}, u32[]{:S(2)}) copy-start(bf16[2,256,2048]{2,1,0:T(8,128)(2,1)} %param.38) | copy-start | bytes 6291460
  7.2 111.0 %all-gather.6.cloned.1.call-start = ((), (), s32[]{:S(2)}) async-start(), calls=%async_computation.6 | async-start | bytes 6553600 | tf_op jit(solution)/shard_map/all_gather | solution.py:23
  13.9 44.5 %copy-start.6 = (bf16[64,32]{0,1:T(8,128)(2,1)S(1)}, bf16[64,32]{0,1:T(8,128)(2,1)}, u32[]{:S(2)}) copy-start(bf16[64,32]{0,1:T(8,128)(2,1)} %param.24) | copy-start | bytes 12292
  13.9 54.4 %copy-start.4 = (bf16[64,256]{1,0:T(8,128)(2,1)S(1)}, bf16[64,256]{1,0:T(8,128)(2,1)}, u32[]{:S(2)}) copy-start(bf16[64,256]{1,0:T(8,128)(2,1)} %param.23) | copy-start | bytes 98308
  13.9 54.5 %copy-start.8 = (f32[256]{0:T(256)S(1)}, f32[256]{0:T(256)}, u32[]{:S(2)}) copy-start(f32[256]{0:T(256)} %param.26) | copy-start | bytes 3076
  55.3 27.1 %copy-start.3 = (bf16[64,512]{1,0:T(8,128)(2,1)S(1)}, bf16[64,512]{1,0:T(8,128)(2,1)}, u32[]{:S(2)}) copy-start(bf16[64,512]{1,0:T(8,128)(2,1)} %param.22) | copy-start | bytes 196612
  55.3 27.2 %copy-start.7 = (f32[512]{0:T(512)S(1)}, f32[512]{0:T(512)}, u32[]{:S(2)}) copy-start(f32[512]{0:T(512)} %param.25) | copy-start | bytes 6148
  58.3 150.4 %all-gather.4.cloned.1.call-start = ((), (), s32[]{:S(2)}) async-start(), calls=%async_computation.5 | async-start | bytes 9584640 | tf_op jit(solution)/shard_map/all_gather | solution.py:34
  82.3 194.1 %reduce-scatter.3.cloned.1.call-start = ((), (), s32[]{:S(2)}) async-start(), calls=%async_computation.7 | async-start | bytes 5242880 | tf_op jit(solution)/shard_map/reduce_scatter | solution.py:264
  223.6 4.3 %slice-start = ((bf16[16384,288]{0,1:T(8,128)(2,1)}), bf16[16384,32]{0,1:T(8,128)(2,1)S(1)}, s32[]{:S(2)}) async-start(bf16[16384,288]{0,1:T(8,128)(2,1)} %all-gather.4.cloned.1.call-done), calls=%async_computation.9 | async-start | bytes 2097152 | tf_op jit(solution)/shard_map/split | solution.py:34
  228.0 40.7 %copy-start.2 = (bf16[128,2048]{1,0:T(8,128)(2,1)S(1)}, bf16[128,2048]{1,0:T(8,128)(2,1)}, u32[]{:S(2)}) copy-start(bf16[128,2048]{1,0:T(8,128)(2,1)} %param.31) | copy-start | bytes 1572868
  270.2 29.9 %copy-start.10 = (bf16[256,2048]{1,0:T(8,128)(2,1)S(1)}, bf16[256,2048]{1,0:T(8,128)(2,1)}, u32[]{:S(2)}) copy-start(bf16[256,2048]{1,0:T(8,128)(2,1)} %param.41) | copy-start | bytes 3145732
  270.2 18.8 %all-to-all-start = ((bf16[4,64,2048]{2,1,0:T(8,128)(2,1)}), bf16[4,64,2048]{2,1,0:T(8,128)(2,1)S(1)}, u32[]{:S(2)}, u32[]{:S(2)}) async-start(bf16[4,64,2048]{2,1,0:T(8,128)(2,1)} %bitcast.10), calls=%async_computation | async-start | bytes 2097152 | tf_op jit(solution)/shard_map/all_to_all | solution.py:44
  279.6 24.4 %copy-start.5 = (s32[64,2]{0,1:T(2,128)S(1)}, s32[64,2]{0,1:T(2,128)}, u32[]{:S(2)}) copy-start(s32[64,2]{0,1:T(2,128)} %param.34) | copy-start | bytes 1540
  279.6 24.6 %copy-start.9 = (f32[64,2]{0,1:T(2,128)S(1)}, f32[64,2]{0,1:T(2,128)}, u32[]{:S(2)}) copy-start(f32[64,2]{0,1:T(2,128)} %param.35) | copy-start | bytes 1540
  289.0 39.2 %all-to-all-start.2 = ((bf16[64,2,2,2048]{3,2,1,0:T(2,128)(2,1)}), bf16[64,2,2,2048]{3,2,1,0:T(2,128)(2,1)}, u32[]{:S(2)}, u32[]{:S(2)}) async-start(bf16[64,2,2,2048]{3,2,1,0:T(2,128)(2,1)} %copy.87), calls=%async_computation.3 | async-start | bytes 2097152 | tf_op jit(solution)/shard_map/all_to_all | solution.py:272
  300.1 35.3 %reduce-scatter.5.cloned.1.call-start = ((), (), s32[]{:S(2)}) async-start(), calls=%async_computation.8 | async-start | bytes 1310720 | tf_op jit(solution)/shard_map/reduce_scatter | solution.py:267
  328.2 9.0 %copy-start.1 = (bf16[2,256,2048]{2,1,0:T(8,128)(2,1)S(1)}, bf16[2,256,2048]{2,1,0:T(8,128)(2,1)}, u32[]{:S(2)}) copy-start(bf16[2,256,2048]{2,1,0:T(8,128)(2,1)} %param.38) | copy-start | bytes 6291460
Sparse Core Ops, SparseCore 0:
  58.5 59.7 all-gather.5
  121.4 87.2 all-gather.3
  211.3 49.7 reduce-scatter.2
  304.1 23.9 reduce-scatter.4
where the time goes:
time: 345 us; the launch traced here: 344 us
  waiting for transfers between devices  119 us (34%)
  blocking collectives  74.1 us (21%)
  matrix products  60.6 us (18%)
  local copies, waits for them, and re-layouts  43.4 us (13%)
  other arithmetic  16 us (5%)
  starting transfers between devices  15.4 us (4%)
  between operations  14.2 us (4%)
    all_gather x1, waiting for transfers between devices, sent_together(): lax.all_gather(both, axis, axis=dim, tiled=True)  66.4 us
    all_to_all x1, blocking collectives, shards(): lax.all_to_all(outgoing, 'ep', split_axis=0, concat_axis=0, tiled=True)  41.4 us
    all_to_all x1, waiting for transfers between devices, shards(): lax.all_to_all(routed_sum.astype(jnp.bfloat16), 'ep', split_axis=0, conca...  22.7 us
    unnamed x30, local copies, waits for them, and re-layouts  22.4 us
    all_gather x1, waiting for transfers between devices, side_by_side(): out = lax.all_gather(both, axis, axis=dim, tiled=True)  20.7 us
    dot_general x8, matrix products, absorb_block(): jnp.einsum('qhk,khv->qhv', weights.astype(jnp.bfloat16), value_rows, pref...  14.8 us
    dot_general x8, matrix products, absorb_block(): jnp.einsum('qhc,khc->qhk', query_part, key_part, preferred_element_type=j...  14.5 us
    all_gather x1, blocking collectives, shards(): lax.all_gather(query_normed, 'tp', axis=0, tiled=True)  12.3 us
  transfers between devices with their start and end apart: 6, of which 4 were waited for; matrix products, arithmetic and copies ran while one was open for 32% of the time, Pallas kernels for 0%

commit v1 on v0

v1 whole, which is shorter than its diff:
```python
import functools
import math

import jax
import jax.numpy as jnp
from jax import lax
from jax.experimental import pallas as pl
from jax.experimental.pallas import tpu as pltpu
from jax.sharding import PartitionSpec as P

MESH = pl.DeviceIdType.MESH
F32 = jnp.float32
BF16 = jnp.bfloat16

HEADS = 8
CONTENT = 64
ROTARY = 32
VALUE = 64
NZ, NX, NC, NY = 8, 4, 2, 4
NXC = NX * NC
ROWS = 64
GROUP = ROWS * NY
D = 2048
CH = 4
CW = D // CH
LAT = 512 + 256 + 128
norm_eps = 1e-06
rope_base = 10000.0
EXP_SCALE = (CONTENT + ROTARY) ** (-0.5) * math.log2(math.e)


def mm(a, b):
    return jnp.dot(a, b, preferred_element_type=F32)


def mm_nt(a, b):
    return lax.dot_general(a, b, (((1,), (1,)), ((), ())), preferred_element_type=F32)


def kernel(
    lat_ref, tok_ref, routes_ref, rw_ref, cos_ref, sin_ref,
    wq_ref, wr_ref, ws_ref, wk_ref, wv_ref, wo_ref,
    gate_hbm, up_hbm, down_hbm, sgate_hbm, sup_hbm, sdown_hbm,
    mix_ref, exp_ref,
    gate_v, up_v, down_v, sgate_v, sup_v, sdown_v, wsem,
    latg, tokg, s1, r1, s2, g, acc, hid, part, rsa, rsb, s3, r3, s4, r4,
    qg, kg, vg, st, osend, ssend, orecv, srecv,
    psh, sha, shb, ssum, pmx, mxa, mxb,
    send_sem, recv_sem,
):
    ep = lax.axis_index("ep")
    y = lax.axis_index("tp")
    z = ep // NXC
    xc = lax.rem(ep, NXC)
    x = xc // NC
    core = lax.rem(xc, NC)
    yp, ym, ya = lax.rem(y + 1, NY), lax.rem(y + NY - 1, NY), lax.rem(y + 2, NY)
    xp, xm, xa = lax.rem(x + 1, NX), lax.rem(x + NX - 1, NX), lax.rem(x + 2, NX)
    xcp, xcm, xca = xp * NC + core, xm * NC + core, xa * NC + core
    mate = x * NC + (1 - core)
    zs = [lax.rem(z + d, NZ) for d in range(NZ)]
    xcs = [lax.rem(xc + d, NXC) for d in range(NXC)]

    used = [0]
    waits = []

    def sems():
        used[0] += 1
        return send_sem.at[used[0] - 1], recv_sem.at[used[0] - 1]

    def remote(src, dst, pair, e, t):
        return pltpu.make_async_remote_copy(
            src_ref=src, dst_ref=dst, send_sem=pair[0], recv_sem=pair[1],
            device_id=(e, t), device_id_type=MESH,
        )

    def send(src, dst, e, t):
        copy = remote(src, dst, sems(), e, t)
        copy.start()
        waits.append(copy.wait_send)
        return copy

    def whole_wait(ref, sem):
        pltpu.make_async_copy(ref, ref, sem).wait()

    loads = []
    for k, (src, dst) in enumerate([
        (gate_hbm, gate_v), (up_hbm, up_v), (down_hbm, down_v),
        (sgate_hbm, sgate_v), (sup_hbm, sup_v), (sdown_hbm, sdown_v),
    ]):
        copy = pltpu.make_async_copy(src, dst, wsem.at[k])
        copy.start()
        loads.append(copy)

    barrier = pltpu.get_barrier_semaphore()
    for d in range(1, NZ):
        pl.semaphore_signal(barrier, inc=1, device_id=(zs[d] * NXC + xc, y), device_id_type=MESH)
    for d in range(1, NXC):
        pl.semaphore_signal(barrier, inc=1, device_id=(z * NXC + xcs[d], y), device_id_type=MESH)
    for t in (yp, ym):
        pl.semaphore_signal(barrier, inc=1, device_id=(ep, t), device_id_type=MESH)
    pl.semaphore_wait(barrier, NZ - 1 + NXC - 1 + 2)

    def gather_start(src, buf):
        return [send(src, buf.at[y], ep, yp), send(src, buf.at[y], ep, ym)]

    def gather_forward(first, buf):
        first[0].wait_recv()
        a = send(buf.at[ym, 0], buf.at[ym, 0], ep, yp)
        first[1].wait_recv()
        b = send(buf.at[yp, 1], buf.at[yp, 1], ep, ym)
        return [a, b]

    def gather_finish(second):
        second[0].wait_recv()
        second[1].wait_recv()

    def reduce_start(parts, far):
        return [
            send(parts.at[ya, 0], far.at[0], ep, yp),
            send(parts.at[ya, 1], far.at[1], ep, ym),
        ]

    def reduce_forward(first, parts, far, near):
        first[0].wait_recv()
        parts[yp, 0] = (parts[yp, 0].astype(F32) + far[0].astype(F32)).astype(BF16)
        a = send(parts.at[yp], near.at[0], ep, yp)
        first[1].wait_recv()
        parts[ym, 1] = (parts[ym, 1].astype(F32) + far[1].astype(F32)).astype(BF16)
        b = send(parts.at[ym], near.at[1], ep, ym)
        return [a, b]

    def reduce_finish(second, parts, near):
        second[0].wait_recv()
        second[1].wait_recv()
        return parts[y].astype(F32) + near[0].astype(F32) + near[1].astype(F32)

    def exchange_z(c, src, dst):
        pair = sems()
        for d in (4, 3, 5, 2, 6, 1, 7):
            remote(src.at[c, zs[d]], dst.at[c, z], pair, zs[d] * NXC + xc, y).start()
        dst[c, z] = src[c, z]
        waits.append(functools.partial(whole_wait, dst.at[c, pl.ds(0, NZ - 1)], pair[0]))
        return functools.partial(whole_wait, dst.at[c, pl.ds(0, NZ - 1)], pair[1])

    lat_first = gather_start(lat_ref, latg)
    latg[y] = lat_ref[...]

    r0 = routes_ref[0:1, :].astype(F32)
    r1_row = routes_ref[1:2, :].astype(F32)
    i_row = lax.broadcasted_iota(jnp.int32, (ROWS, ROWS), 0)
    i_col = lax.broadcasted_iota(jnp.int32, (ROWS, ROWS), 1)
    eye = i_row == i_col
    before = i_row < i_col

    def as_column(row):
        return jnp.sum(jnp.where(eye, row, 0.0), axis=1, keepdims=True)

    c0, c1 = as_column(r0), as_column(r1_row)

    def target(row):
        hits = jnp.where(before & ((c0 == row) | (c1 == row)), 1.0, 0.0)
        return row * 2.0 + jnp.sum(hits, axis=0, keepdims=True)

    t0, t1 = target(r0), target(r1_row)
    slot = lax.broadcasted_iota(jnp.int32, (256, ROWS), 0).astype(F32)
    picker = jnp.where((slot == t0) | (slot == t1), 1.0, 0.0).astype(BF16)
    slot_t = lax.broadcasted_iota(jnp.int32, (ROWS, 256), 1).astype(F32)
    select = [
        jnp.where(slot_t == as_column(t), 1.0, 0.0).astype(BF16) for t in (t0, t1)
    ]
    share = [as_column(rw_ref[k : k + 1, :]) for k in range(2)]

    z_wait = []
    for c in range(CH):
        tok_c = tok_ref[:, :, c * CW : (c + 1) * CW].reshape(ROWS, CW)
        s1[c] = mm(picker, tok_c).astype(BF16).reshape(NZ, 32, CW)
        z_wait.append(exchange_z(c, s1, r1))
    tok_first = gather_start(tok_ref, tokg)
    tokg[y] = tok_ref[...]

    p_out = lax.broadcasted_iota(jnp.int32, (256, 256), 0)
    p_in = lax.broadcasted_iota(jnp.int32, (256, 256), 1)

    def moved(i):
        return (
            ((i >> 1) & 7) * 32 + (i >> 5) * 4 + ((i >> 4) & 1) * 2 + (i & 1)
        )

    perm = jnp.where(moved(p_out) == p_in, 1.0, 0.0).astype(BF16)
    perm_back = jnp.where(moved(p_in) == p_out, 1.0, 0.0).astype(BF16)

    lat_second = gather_forward(lat_first, latg)
    gather_finish(lat_second)
    lat = latg[...].reshape(GROUP, LAT)
    qn = lat[:, :512]
    ln = lat[:, 512:768]
    kt = lat[:, 768:]
    turned = (mm(qn, wr_ref[...]) * cos_ref[...] + mm(qn, ws_ref[...]) * sin_ref[...]).astype(BF16)
    qq = mm(qn, wq_ref[...]).astype(BF16) + turned
    kk = mm(ln, wk_ref[...]).astype(BF16)
    vt = mm_nt(wv_ref[...], ln).astype(BF16)
    for h in range(2):
        qg[z, h] = qq[:, h * 128 : (h + 1) * 128]
        kg[xc, h] = kk[:, h * 128 : (h + 1) * 128] + kt
        vg[xc, h] = vt[h * 64 : (h + 1) * 64]

    def send_kv(slot_at, halves, e):
        if halves is None:
            return [
                send(kg.at[slot_at], kg.at[slot_at], e, y),
                send(vg.at[slot_at], vg.at[slot_at], e, y),
            ]
        return [
            send(kg.at[slot_at, halves], kg.at[slot_at, halves], e, y),
            send(vg.at[slot_at, halves], vg.at[slot_at, halves], e, y),
        ]

    def wait_kv(copies):
        for copy in copies:
            copy.wait_recv()

    ep_xp, ep_xm, ep_mate = z * NXC + xcp, z * NXC + xcm, z * NXC + mate
    kv_first = [send_kv(xc, None, ep_xp), send_kv(xc, None, ep_xm)]
    kv_mate = [send_kv(xc, None, ep_mate)]
    z_up, z_down = zs[1] * NXC + xc, zs[NZ - 1] * NXC + xc
    q_up = [send(qg.at[z], qg.at[z], z_up, y)]
    q_down = [send(qg.at[z], qg.at[z], z_down, y)]

    def q_forward(step):
        q_up[step - 1].wait_recv()
        if step < 4:
            at = zs[NZ - step]
            q_up.append(send(qg.at[at], qg.at[at], z_up, y))
        if step < 4:
            q_down[step - 1].wait_recv()
            if step < 3:
                at = zs[step]
                q_down.append(send(qg.at[at], qg.at[at], z_down, y))

    def kv_forward():
        wait_kv(kv_first[0])
        second = send_kv(xcm, 0, ep_xp)
        kv_mate.append(send_kv(xcm, None, ep_mate))
        wait_kv(kv_first[1])
        second2 = send_kv(xcp, 1, ep_xm)
        kv_mate.append(send_kv(xcp, None, ep_mate))
        kv_first.append(second)
        kv_first.append(second2)

    def kv_last():
        wait_kv(kv_first[2])
        wait_kv(kv_first[3])
        kv_mate.append(send_kv(xca, None, ep_mate))

    def kv_finish():
        for copies in kv_mate:
            wait_kv(copies)

    o_pair, st_pair = sems(), sems()

    def attend(d):
        at = zs[d]
        for h in range(2):
            qh = qg[at, h]
            peak = None
            for k in range(NXC):
                s = mm_nt(kg[k, h], qh)
                st[h, k] = s
                top = jnp.max(s, axis=0, keepdims=True)
                peak = top if peak is None else jnp.maximum(peak, top)
            total = jnp.zeros((1, GROUP), F32)
            out = jnp.zeros((VALUE, GROUP), F32)
            for k in range(NXC):
                w = jnp.exp2((st[h, k] - peak) * EXP_SCALE)
                total = total + jnp.sum(w, axis=0, keepdims=True)
                out = out + mm(vg[k, h], w.astype(BF16))
            result = (out / total).astype(BF16)
            level = peak * EXP_SCALE + jnp.log2(total)
            if d == 0:
                orecv[z, h * 64 : (h + 1) * 64] = result
                srecv[z, h : h + 1] = level
            else:
                osend[d - 1, h * 64 : (h + 1) * 64] = result
                ssend[d - 1, h : h + 1] = level
        if d:
            e = at * NXC + xc
            remote(osend.at[d - 1], orecv.at[z], o_pair, e, y).start()
            remote(ssend.at[d - 1], srecv.at[z], st_pair, e, y).start()

    def project():
        whole_wait(orecv.at[pl.ds(0, NZ - 1)], o_pair[1])
        whole_wait(srecv.at[pl.ds(0, NZ - 1)], st_pair[1])
        waits.append(functools.partial(whole_wait, osend, o_pair[0]))
        waits.append(functools.partial(whole_wait, ssend, st_pair[0]))
        rows = []
        for h in range(2):
            levels = [srecv[k, h : h + 1] for k in range(NZ)]
            top = functools.reduce(jnp.maximum, levels)
            scaled = [jnp.exp2(v - top) for v in levels]
            total = functools.reduce(lambda a, b: a + b, scaled)
            summed = functools.reduce(
                lambda a, b: a + b,
                [orecv[k, h * 64 : (h + 1) * 64].astype(F32) * scaled[k] for k in range(NZ)],
            )
            rows.append(summed / total)
        attended = jnp.concatenate(rows, axis=0).T.astype(BF16)
        for c in range(CH):
            pmx[:, :, :, c * CW : (c + 1) * CW] = (
                mm(attended, wo_ref[:, c * CW : (c + 1) * CW]).astype(BF16).reshape(NY, 2, 32, CW)
            )
        return reduce_start(pmx, mxa)

    xc_pairs = {}

    def to_expert(c):
        z_wait[c]()
        s2[c] = mm(perm, r1[c].reshape(256, CW)).astype(BF16).reshape(NXC, 32, CW)
        pair = sems()
        for d in (4, 2, 6, 3, 5, 7, 1):
            remote(s2.at[c, xcs[d]], g.at[c, y, xc // 4, lax.rem(xc, 4)], pair, z * NXC + xcs[d], y).start()
        g[c, y, xc // 4, lax.rem(xc, 4)] = s2[c, xc]
        waits.append(functools.partial(whole_wait, s2.at[c, pl.ds(0, NXC - 1)], pair[0]))
        xc_pairs[c] = pair

    g_first, g_second = {}, {}

    def spread(c):
        whole_wait(s2.at[c, pl.ds(0, NXC - 1)], xc_pairs[c][1])
        g_first[c] = [
            send(g.at[c, y], g.at[c, y], ep, yp), send(g.at[c, y], g.at[c, y], ep, ym)
        ]

    def spread_on(c):
        g_second[c] = gather_forward(g_first[c], g.at[c])

    def lift(c):
        gather_finish(g_second[c])
        if c == 0:
            for k in (0, 1):
                loads[k].wait()
        for e in range(2):
            rows = g[c, :, :, :, e * 16 : (e + 1) * 16, :].reshape(512, CW)
            for j, w in enumerate((gate_v, up_v)):
                term = mm(rows, w[e, c * CW : (c + 1) * CW, :])
                acc[e, j] = term if c == 0 else acc[e, j] + term

    def activate():
        loads[2].wait()
        for e in range(2):
            v = acc[e, 0]
            hid[e] = (v / (1.0 + jnp.exp(-v)) * acc[e, 1]).astype(BF16)

    p_first, p_second, x_back, z_back = {}, {}, {}, {}

    def lower(c):
        for e in range(2):
            part[c, :, :, :, e * 16 : (e + 1) * 16, :] = (
                mm(hid[e], down_v[e, :, c * CW : (c + 1) * CW]).astype(BF16).reshape(NY, 2, 4, 16, CW)
            )
        p_first[c] = reduce_start(part.at[c], rsa.at[c])

    def lower_on(c):
        p_second[c] = reduce_forward(p_first[c], part.at[c], rsa.at[c], rsb.at[c])

    def back_x(c):
        s3[c] = reduce_finish(p_second[c], part.at[c], rsb.at[c]).astype(BF16).reshape(NXC, 32, CW)
        pair = sems()
        for d in (4, 2, 6, 3, 5, 7, 1):
            remote(s3.at[c, xcs[d]], r3.at[c, xc], pair, z * NXC + xcs[d], y).start()
        r3[c, xc] = s3[c, xc]
        waits.append(functools.partial(whole_wait, s3.at[c, pl.ds(0, NXC - 1)], pair[0]))
        x_back[c] = pair

    def back_z(c):
        whole_wait(s3.at[c, pl.ds(0, NXC - 1)], x_back[c][1])
        s4[c] = mm(perm_back, r3[c].reshape(256, CW)).astype(BF16).reshape(NZ, 32, CW)
        z_back[c] = exchange_z(c, s4, r4)

    def combine(c):
        z_back[c]()
        rows = r4[c].reshape(256, CW)
        routed = share[0] * mm(select[0], rows) + share[1] * mm(select[1], rows)
        exp_ref[:, c * CW : (c + 1) * CW] = (
            routed + ssum[:, :, c * CW : (c + 1) * CW].reshape(ROWS, CW)
        ).astype(BF16)

    def shared():
        for k in (3, 4, 5):
            loads[k].wait()
        rows = tokg[...].reshape(GROUP, D)
        gated = mm(rows, sgate_v[...])
        lifted = mm(rows, sup_v[...])
        hidden = (gated / (1.0 + jnp.exp(-gated)) * lifted).astype(BF16)
        for c in range(CH):
            psh[:, :, :, c * CW : (c + 1) * CW] = (
                mm(hidden, sdown_v[:, c * CW : (c + 1) * CW]).astype(BF16).reshape(NY, 2, 32, CW)
            )

    to_expert(0)
    kv_forward()
    spread(0)
    q_forward(1)
    to_expert(1)
    kv_last()
    tok_second = gather_forward(tok_first, tokg)
    spread(1)
    spread_on(0)
    q_forward(2)
    to_expert(2)
    kv_finish()
    attend(0)
    spread(2)
    spread_on(1)
    q_forward(3)
    to_expert(3)
    attend(1)
    spread(3)
    lift(0)
    spread_on(2)
    q_forward(4)
    attend(7)
    lift(1)
    spread_on(3)
    gather_finish(tok_second)
    shared()
    sh_first = reduce_start(psh, sha)
    attend(2)
    attend(6)
    lift(2)
    lift(3)
    activate()
    lower(0)
    lower(1)
    lower(2)
    lower(3)
    lower_on(0)
    attend(3)
    lower_on(1)
    sh_second = reduce_forward(sh_first, psh, sha, shb)
    back_x(0)
    lower_on(2)
    attend(5)
    back_z(0)
    back_x(1)
    lower_on(3)
    attend(4)
    ssum[...] = reduce_finish(sh_second, psh, shb)
    back_z(1)
    back_x(2)
    mx_first = project()
    back_z(2)
    back_x(3)
    combine(0)
    mx_second = reduce_forward(mx_first, pmx, mxa, mxb)
    back_z(3)
    combine(1)
    combine(2)
    mix_ref[...] = reduce_finish(mx_second, pmx, mxb).reshape(ROWS, D).astype(BF16)
    combine(3)
    for wait in waits:
        wait()


N_SEMS = 160


def fused(*args):
    vmem = pl.BlockSpec(memory_space=pltpu.VMEM)
    hbm = pl.BlockSpec(memory_space=pl.ANY)
    s = lambda *shape: pltpu.VMEM(shape, BF16)
    f = lambda *shape: pltpu.VMEM(shape, F32)
    return pl.pallas_call(
        kernel,
        out_shape=[jax.ShapeDtypeStruct((ROWS, D), BF16)] * 2,
        in_specs=[vmem] * 12 + [hbm] * 6,
        out_specs=[vmem] * 2,
        scratch_shapes=[
            s(2, D, 256), s(2, D, 256), s(2, 256, D), s(D, 256), s(D, 256), s(256, D),
            pltpu.SemaphoreType.DMA((6,)),
            s(NY, 2, 32, LAT), s(NY, 2, 32, D),
            s(CH, NZ, 32, CW), s(CH, NZ, 32, CW), s(CH, NXC, 32, CW),
            s(CH, NY, 2, 4, 32, CW),
            f(2, 2, 512, 256), s(2, 512, 256),
            s(CH, NY, 2, 4, 32, CW), s(CH, 2, 4, 32, CW), s(CH, 2, 2, 4, 32, CW),
            s(CH, NXC, 32, CW), s(CH, NXC, 32, CW), s(CH, NZ, 32, CW), s(CH, NZ, 32, CW),
            s(NZ, 2, GROUP, 128), s(NXC, 2, GROUP, 128), s(NXC, 2, VALUE, GROUP),
            f(2, NXC, GROUP, GROUP),
            s(NZ - 1, 128, GROUP), f(NZ - 1, 8, GROUP), s(NZ, 128, GROUP), f(NZ, 8, GROUP),
            s(NY, 2, 32, D), s(2, 32, D), s(2, 2, 32, D), f(2, 32, D),
            s(NY, 2, 32, D), s(2, 32, D), s(2, 2, 32, D),
            pltpu.SemaphoreType.DMA((N_SEMS,)), pltpu.SemaphoreType.DMA((N_SEMS,)),
        ],
        compiler_params=pltpu.CompilerParams(
            collective_id=0, has_side_effects=True, vmem_limit_bytes=60 * 1024 * 1024
        ),
        name="fused",
    )(*args)


def rms_rows(entries, gain_row):
    widened = entries.astype(F32)
    return widened * lax.rsqrt(jnp.mean(widened * widened, -1, keepdims=True) + norm_eps) * gain_row


def apart(columns, width, at):
    depth = columns.shape[0]
    blocks = columns.reshape(depth, 2, width)
    return jnp.pad(blocks, ((0, 0), (0, 0), (at, 128 - at - width))).reshape(depth, 256)


def halves(columns):
    blocks = columns.reshape(columns.shape[0], -1, ROTARY // 2, 2)
    even, odd = blocks[..., 0], blocks[..., 1]
    return jnp.concatenate([even, odd], -1), jnp.concatenate([odd, even], -1)


def shards(
    query_latent, key_latent, rotary_key, query_gain, latent_gain, query_content, query_rotary,
    key_content, value_weight, output_weight, expert_input, norm_gain, routes, route_weight,
    expert_gate, expert_up, expert_down, shared_gate, shared_up, shared_down,
):
    y = lax.axis_index("tp")
    start = lax.axis_index("ep") * GROUP
    qn = rms_rows(query_latent, query_gain).astype(BF16)
    ln = rms_rows(key_latent, latent_gain).astype(BF16)
    en = rms_rows(expert_input, norm_gain).astype(BF16)
    frequency = rope_base ** (-jnp.arange(ROTARY // 2, dtype=F32) * 2.0 / ROTARY)
    angles = (start + jnp.arange(GROUP, dtype=jnp.int32)).astype(F32)[:, None] * frequency[None, :]
    cosine, sine = jnp.cos(angles), jnp.sin(angles)
    cos2 = jnp.concatenate([cosine, cosine], -1)
    sin2 = jnp.concatenate([-sine, sine], -1)
    own_cos = lax.dynamic_slice_in_dim(cos2, y * ROWS, ROWS, 0)
    own_sin = lax.dynamic_slice_in_dim(sin2, y * ROWS, ROWS, 0)
    straight, crossed = halves(rotary_key.astype(F32))
    kt = (straight[:, 0] * own_cos + crossed[:, 0] * own_sin).astype(BF16)
    kt = jnp.pad(kt, ((0, 0), (CONTENT, 128 - CONTENT - ROTARY)))
    lat = jnp.concatenate([qn, ln, kt], -1).reshape(2, 32, LAT)
    spread = lambda t: jnp.pad(t, ((0, 0), (CONTENT, 128 - CONTENT - ROTARY)))
    cos_wide = jnp.tile(spread(cos2), (1, 2))
    sin_wide = jnp.tile(spread(sin2), (1, 2))
    cut = lambda w, width: lax.dynamic_slice_in_dim(w, y * 2 * width, 2 * width, 1)
    wq = apart(cut(query_content, CONTENT), CONTENT, 0)
    wr, ws = halves(cut(query_rotary, ROTARY))
    wr, ws = apart(wr, ROTARY, CONTENT), apart(ws, ROTARY, CONTENT)
    wk = apart(cut(key_content, CONTENT), CONTENT, 0)
    wv = cut(value_weight, VALUE).T
    mix, out = fused(
        lat, en.reshape(2, 32, D), routes.T, route_weight.T, cos_wide, sin_wide,
        wq, wr, ws, wk, wv, output_weight,
        expert_gate, expert_up, expert_down, shared_gate, shared_up, shared_down,
    )
    return mix, out


def solution(mesh):
    both = P(("ep", "tp"), None)
    in_specs = (
        both, both, both, P(), P(), P(), P(), P(), P(), P("tp", None), both, P(), both, both,
        P("ep", None, "tp"), P("ep", None, "tp"), P("ep", "tp", None),
        P(None, "tp"), P(None, "tp"), P("tp", None),
    )
    return jax.shard_map(
        shards, mesh=mesh, in_specs=in_specs, out_specs=(both, both), check_vma=False
    )
```

time: 345 us -> 157 us (0.46)
  Pallas kernels: 0 us -> 136 us
  waiting for transfers between devices: 119 us -> 0 us
  blocking collectives: 74.1 us -> 0 us
  matrix products: 60.6 us -> 0 us
  local copies, waits for them, and re-layouts: 43.4 us -> 12.7 us
  starting transfers between devices: 15.4 us -> 0 us
  between operations: 14.2 us -> 0.85 us
  other arithmetic: 16 us -> 6.63 us
    pallas_call x0 -> x1, Pallas kernels: none -> 136 us  [fused(): pl.pallas_call(kernel, out_shape=[jax.ShapeDtypeStruct((ROWS, D), BF16)]...]
    all_gather x2 -> x0, waiting for transfers between devices: 87.1 us -> none  [the longest x1 66.4 us: sent_together(): lax.all_gather(both, axis, axis=dim, tiled=True)]
    dot_general x34 -> x0, matrix products: 60.6 us -> none  [the longest x8 14.8 us: absorb_block(): jnp.einsum('qhk,khv->qhv', weights.astype(jnp.bfloat16), value_rows, pref...]
    all_to_all x1 -> x0, blocking collectives: 41.4 us -> none  [shards(): lax.all_to_all(outgoing, 'ep', split_axis=0, concat_axis=0, tiled=True)]
    all_gather x3 -> x0, blocking collectives: 32.7 us -> none  [the longest x1 12.3 us: shards(): lax.all_gather(query_normed, 'tp', axis=0, tiled=True)]
    all_to_all x2 -> x0, waiting for transfers between devices: 32 us -> none  [the longest x1 22.7 us: shards(): lax.all_to_all(routed_sum.astype(jnp.bfloat16), 'ep', split_axis=0, conca...]
    unnamed x30 -> x17, local copies, waits for them, and re-layouts: 22.4 us -> 6.03 us
    all_to_all x2 -> x0, starting transfers between devices: 15.2 us -> none  [the longest x1 11.1 us: shards(): lax.all_to_all(routed_sum.astype(jnp.bfloat16), 'ep', split_axis=0, conca...]
  transfers between devices with their start and end apart: 6 -> 0, of which waited for: 4 -> 0; matrix products, arithmetic and copies ran while one was open for 32% -> 0% of each run, Pallas kernels for 0% -> 0%
where the time goes in v1:
time: 157 us; the launch traced here: 156 us
  Pallas kernels  136 us (87%)
  local copies, waits for them, and re-layouts  12.7 us (8%)
  other arithmetic  6.63 us (4%)
    pallas_call x1, Pallas kernels, fused(): pl.pallas_call(kernel, out_shape=[jax.ShapeDtypeStruct((ROWS, D), BF16)]...  136 us
    unnamed x17, local copies, waits for them, and re-layouts  6.03 us
    reshape x4, local copies, waits for them, and re-layouts, apart(): jnp.pad(blocks, ((0, 0), (0, 0), (at, 128 - at - width)))  3.27 us

profile of v1, /device:TPU:1, one launch (start us, length us, event | category | flops | bytes accessed | tf_op | source)
XLA Modules:
  0.0 156.1 jit_solution(1611482351198573629)
XLA Ops:
  0.7 1.0 fusion.8
  1.7 0.9 fusion.12
  2.6 1.1 fusion
  3.7 0.8 fusion.23
  4.5 0.8 fusion.14
  5.4 0.1 multiply_cosine_fusion
  5.6 0.1 copy.89
  5.7 0.9 fusion.10
  6.6 0.7 fusion.11
  7.4 0.1 copy.90
  7.5 0.1 pad.27.clone
  7.6 1.0 constant_dynamic-slice_fusion.1
  8.6 0.1 copy.73
  8.7 0.1 fusion.22
  8.9 0.1 tile.8
  9.0 0.7 copy.99
  9.7 0.1 copy.91
  9.8 0.1 pad.28.clone
  9.9 0.1 tile.20
  10.0 0.7 copy.98
  10.7 0.1 copy.86
  10.9 0.9 constant_dynamic-slice_fusion
  11.7 0.1 copy.87
  11.9 0.8 copy.82.wk_ref
  12.6 0.7 copy.88
  13.4 0.8 copy.79.wq_ref
  14.2 0.8 fusion.2
  15.1 0.8 copy.81.ws_ref
  16.0 0.8 copy.80.wr_ref
  16.8 136.0 %fused.1 = (bf16[64,2048]{1,0:T(8,128)(2,1)}, bf16[64,2048]{1,0:T(8,128)(2,1)}) custom-call(bf16[2,32,896]{2,1,0:T(8,128)(2,1)} %bitcast.49, bf16[2,32,2048]{2,1,0:T(8,128)(2,1)} %bitcast.39, s32[2,64]{1,0:T(2,128)} %bitcast.55, f32[2,64]{1,0:T(2,128)} %bitcast.56, f32[256,256]{1,0:T(8,128)} %bitcast.40, f32[256,256]{1,0:T(8,128)} %bitcast.41, ...), custom_call_target="tpu_custom_call" | custom-call | tf_op jit(solution)/shard_map/fused/pallas_call | solution.py:473
  152.8 1.7 %copy.102 = bf16[64,2048]{1,0:T(8,128)(2,1)} copy(bf16[64,2048]{1,0:T(8,128)(2,1)} %get-tuple-element.19) | data formatting | bytes 524288
  154.5 1.7 %copy.103 = bf16[64,2048]{1,0:T(8,128)(2,1)} copy(bf16[64,2048]{1,0:T(8,128)(2,1)} %get-tuple-element.20) | data formatting | bytes 524288
  (19 shorter events, 0.3 us)
Async XLA Ops:
  0.6 10.1 %copy-start = (bf16[512,512]{1,0:T(8,128)(2,1)S(1)}, bf16[512,512]{1,0:T(8,128)(2,1)}, u32[]{:S(2)}) copy-start(bf16[512,512]{1,0:T(8,128)(2,1)} %param.25) | copy-start | bytes 1572868
  9.0 5.3 %copy-start.1 = (bf16[64,2048]{1,0:T(8,128)(2,1)S(1)}, bf16[64,2048]{1,0:T(8,128)(2,1)}, u32[]{:S(2)}) copy-start(bf16[64,2048]{1,0:T(8,128)(2,1)} %param.30) | copy-start | bytes 786436
  9.0 5.3 %copy-start.2 = (f32[2048]{0:T(1024)S(1)}, f32[2048]{0:T(1024)}, u32[]{:S(2)}) copy-start(f32[2048]{0:T(1024)} %param.31) | copy-start | bytes 24580

commit v2 on v1

--- a/solution.py
+++ b/solution.py
@@ -3,6 +3,7 @@
 
 import jax
 import jax.numpy as jnp
+import numpy as np
 from jax import lax
 from jax.experimental import pallas as pl
 from jax.experimental.pallas import tpu as pltpu
@@ -21,13 +22,21 @@
 ROWS = 64
 GROUP = ROWS * NY
 D = 2048
-CH = 4
+CH = 8
 CW = D // CH
 LAT = 512 + 256 + 128
 norm_eps = 1e-06
 rope_base = 10000.0
 EXP_SCALE = (CONTENT + ROTARY) ** (-0.5) * math.log2(math.e)
 
+ORDER = " ".join([
+    "X.0 G X.1 Y.0 P X.2 Y.1 X.3 F.0 Y.2 X.4 F.1 Y.3 K X.5 F.2 Y.4 X.6 F.3 Y.5 K2 X.7 F.4 Y.6 T Y.7 F.5 K3",
+    "A.0 F.6 S L.0 L.1 Q.1 A.1 F.7 S2 L.2 L.3 L.4 L.5 L.6 L.7 V",
+    "W.0 W.1 W.2 A.7 W2.0 W.3 Q.2 A.2 W2.1 W.4 A.6 W2.2 B.0 W.5 Q.3 A.3 W2.3 B.1 Z.0 W.6 A.5",
+    "W2.4 B.2 Z.1 W.7 Q.4 A.4 S3 W2.5 B.3 Z.2 C.0 W2.6 B.4 Z.3 C.1 W2.7 M B.5 Z.4 C.2 B.6 Z.5 C.3 B.7 Z.6 M2",
+    "C.4 C.5 Z.7 C.6 M3 C.7",
+])
+
 
 def mm(a, b):
     return jnp.dot(a, b, preferred_element_type=F32)
@@ -38,11 +47,11 @@
 
 
 def kernel(
-    lat_ref, tok_ref, routes_ref, rw_ref, cos_ref, sin_ref,
-    wq_ref, wr_ref, ws_ref, wk_ref, wv_ref, wo_ref,
+    ql_ref, kl_ref, rk_ref, qgain_ref, lgain_ref, tok_ref, ngain_ref, routes_ref, rw_ref, turn_ref,
+    qc_hbm, qr_hbm, kc_hbm, vw_hbm, wo_hbm,
     gate_hbm, up_hbm, down_hbm, sgate_hbm, sup_hbm, sdown_hbm,
     mix_ref, exp_ref,
-    gate_v, up_v, down_v, sgate_v, sup_v, sdown_v, wsem,
+    gate_v, up_v, down_v, sgate_v, sup_v, sdown_v, qc_v, qr_v, kc_v, vw_v, wo_v, angle, wsem,
     latg, tokg, s1, r1, s2, g, acc, hid, part, rsa, rsb, s3, r3, s4, r4,
     qg, kg, vg, st, osend, ssend, orecv, srecv,
     psh, sha, shb, ssum, pmx, mxa, mxb,
@@ -63,6 +72,7 @@
 
     used = [0]
     waits = []
+    held = {}
 
     def sems():
         used[0] += 1
@@ -82,15 +92,6 @@
 
     def whole_wait(ref, sem):
         pltpu.make_async_copy(ref, ref, sem).wait()
-
-    loads = []
-    for k, (src, dst) in enumerate([
-        (gate_hbm, gate_v), (up_hbm, up_v), (down_hbm, down_v),
-        (sgate_hbm, sgate_v), (sup_hbm, sup_v), (sdown_hbm, sdown_v),
-    ]):
-        copy = pltpu.make_async_copy(src, dst, wsem.at[k])
-        copy.start()
-        loads.append(copy)
 
     barrier = pltpu.get_barrier_semaphore()
     for d in range(1, NZ):
@@ -99,7 +100,18 @@
         pl.semaphore_signal(barrier, inc=1, device_id=(z * NXC + xcs[d], y), device_id_type=MESH)
     for t in (yp, ym):
         pl.semaphore_signal(barrier, inc=1, device_id=(ep, t), device_id_type=MESH)
-    pl.semaphore_wait(barrier, NZ - 1 + NXC - 1 + 2)
+
+    cols = pl.ds(pl.multiple_of(y * 128, 128), 128)
+    loads = []
+    for k, (src, dst) in enumerate([
+        (gate_hbm, gate_v), (up_hbm, up_v), (down_hbm, down_v),
+        (sgate_hbm, sgate_v), (sup_hbm, sup_v), (sdown_hbm, sdown_v),
+        (qc_hbm.at[:, cols], qc_v), (qr_hbm, qr_v), (kc_hbm.at[:, cols], kc_v),
+        (vw_hbm.at[:, cols], vw_v), (wo_hbm, wo_v),
+    ]):
+        loads.append(pltpu.make_async_copy(src, dst, wsem.at[k]))
+    for k in (6, 7, 8, 9, 0, 1, 3, 4, 5, 2, 10):
+        loads[k].start()
 
     def gather_start(src, buf):
         return [send(src, buf.at[y], ep, yp), send(src, buf.at[y], ep, ym)]
@@ -143,8 +155,12 @@
         waits.append(functools.partial(whole_wait, dst.at[c, pl.ds(0, NZ - 1)], pair[0]))
         return functools.partial(whole_wait, dst.at[c, pl.ds(0, NZ - 1)], pair[1])
 
-    lat_first = gather_start(lat_ref, latg)
-    latg[y] = lat_ref[...]
+    def normed(ref, gain_ref):
+        v = ref[...].astype(F32)
+        return (v * lax.rsqrt(jnp.mean(v * v, -1, keepdims=True) + norm_eps) * gain_ref[...]).astype(BF16)
+
+    normed_rows = normed(tok_ref, ngain_ref)
+    tokg[y] = normed_rows.reshape(2, 32, D)
 
     r0 = routes_ref[0:1, :].astype(F32)
     r1_row = routes_ref[1:2, :].astype(F32)
@@ -171,13 +187,45 @@
     ]
     share = [as_column(rw_ref[k : k + 1, :]) for k in range(2)]
 
-    z_wait = []
     for c in range(CH):
-        tok_c = tok_ref[:, :, c * CW : (c + 1) * CW].reshape(ROWS, CW)
-        s1[c] = mm(picker, tok_c).astype(BF16).reshape(NZ, 32, CW)
-        z_wait.append(exchange_z(c, s1, r1))
-    tok_first = gather_start(tok_ref, tokg)
-    tokg[y] = tok_ref[...]
+        s1[c] = mm(picker, normed_rows[:, c * CW : (c + 1) * CW]).astype(BF16).reshape(NZ, 32, CW)
+
+    latg[y, :, :, :512] = normed(ql_ref, qgain_ref).reshape(2, 32, 512)
+    latg[y, :, :, 512:768] = normed(kl_ref, lgain_ref).reshape(2, 32, 256)
+    position = ep * GROUP + lax.broadcasted_iota(jnp.int32, (GROUP, 128), 0)
+    angles = position.astype(F32) * turn_ref[0:1, :]
+    angle[0] = jnp.cos(angles)
+    angle[1] = jnp.sin(angles) * turn_ref[1:2, :]
+
+    def lanes(depth, width):
+        return (
+            lax.broadcasted_iota(jnp.int32, (depth, width), 0),
+            lax.broadcasted_iota(jnp.int32, (depth, width), 1),
+        )
+
+    def one_hot(cond):
+        return jnp.where(cond, 1.0, 0.0).astype(BF16)
+
+    def rotary_source(lane, flip):
+        i = (lane & 127) - CONTENT
+        first = (i & 15) * 2
+        late = i >> 4
+        inside = (i >= 0) & (i < ROTARY)
+        return first + ((1 - late) if flip else late), inside
+
+    src, lane = lanes(ROTARY, 128)
+    pair = []
+    for flip in (False, True):
+        entry, inside = rotary_source(lane, flip)
+        pick = one_hot((src == entry) & inside)
+        pair.append(lax.dot_general(rk_ref[...], pick, (((0,), (0,)), ((), ())), preferred_element_type=F32))
+    own = pl.ds(pl.multiple_of(y * ROWS, ROWS), ROWS)
+    latg[y, :, :, 768:] = (pair[0] * angle[0, own, :] + pair[1] * angle[1, own, :]).astype(BF16).reshape(2, 32, 128)
+
+    pl.semaphore_wait(barrier, NZ - 1 + NXC - 1 + 2)
+    lat_first = gather_start(latg.at[y], latg)
+    z_wait = [exchange_z(c, s1, r1) for c in range(CH)]
+    tok_first = gather_start(tokg.at[y], tokg)
 
     p_out = lax.broadcasted_iota(jnp.int32, (256, 256), 0)
     p_in = lax.broadcasted_iota(jnp.int32, (256, 256), 1)
@@ -190,20 +238,41 @@
     perm = jnp.where(moved(p_out) == p_in, 1.0, 0.0).astype(BF16)
     perm_back = jnp.where(moved(p_in) == p_out, 1.0, 0.0).astype(BF16)
 
-    lat_second = gather_forward(lat_first, latg)
-    gather_finish(lat_second)
-    lat = latg[...].reshape(GROUP, LAT)
-    qn = lat[:, :512]
-    ln = lat[:, 512:768]
-    kt = lat[:, 768:]
-    turned = (mm(qn, wr_ref[...]) * cos_ref[...] + mm(qn, ws_ref[...]) * sin_ref[...]).astype(BF16)
-    qq = mm(qn, wq_ref[...]).astype(BF16) + turned
-    kk = mm(ln, wk_ref[...]).astype(BF16)
-    vt = mm_nt(wv_ref[...], ln).astype(BF16)
-    for h in range(2):
-        qg[z, h] = qq[:, h * 128 : (h + 1) * 128]
-        kg[xc, h] = kk[:, h * 128 : (h + 1) * 128] + kt
-        vg[xc, h] = vt[h * 64 : (h + 1) * 64]
+    def lat_on():
+        held["lat"] = gather_forward(lat_first, latg)
+
+    def queries_keys():
+        gather_finish(held["lat"])
+        for k in (6, 7, 8, 9):
+            loads[k].wait()
+        lat = latg[...].reshape(GROUP, LAT)
+        qn = lat[:, :512]
+        ln = lat[:, 512:768]
+        kt = lat[:, 768:]
+        src, lane = lanes(128, 256)
+        spread_out = one_hot((src == (lane >> 7) * CONTENT + (lane & 127)) & ((lane & 127) < CONTENT))
+        wq = mm(qc_v[...], spread_out).astype(BF16)
+        wk = mm(kc_v[...], spread_out).astype(BF16)
+        src, lane = lanes(256, 256)
+        wide = []
+        for flip in (False, True):
+            entry, inside = rotary_source(lane, flip)
+            pick = one_hot((src == y * 2 * ROTARY + (lane >> 7) * ROTARY + entry) & inside)
+            wide.append(mm(qn, mm(qr_v[...], pick).astype(BF16)))
+        cosine = jnp.concatenate([angle[0], angle[0]], axis=1)
+        sine = jnp.concatenate([angle[1], angle[1]], axis=1)
+        turned = (wide[0] * cosine + wide[1] * sine).astype(BF16)
+        qq = mm(qn, wq).astype(BF16) + turned
+        kk = mm(ln, wk).astype(BF16)
+        vt = mm(ln, vw_v[...]).T.astype(BF16)
+        for h in range(2):
+            qg[z, h] = qq[:, h * 128 : (h + 1) * 128]
+            kg[xc, h] = kk[:, h * 128 : (h + 1) * 128] + kt
+            vg[xc, h] = vt[h * 64 : (h + 1) * 64]
+        kv_first.extend([send_kv(xc, None, ep_xp), send_kv(xc, None, ep_xm)])
+        kv_mate.append(send_kv(xc, None, ep_mate))
+        q_up.append(send(qg.at[z], qg.at[z], z_up, y))
+        q_down.append(send(qg.at[z], qg.at[z], z_down, y))
 
     def send_kv(slot_at, halves, e):
         if halves is None:
@@ -221,11 +290,8 @@
             copy.wait_recv()
 
     ep_xp, ep_xm, ep_mate = z * NXC + xcp, z * NXC + xcm, z * NXC + mate
-    kv_first = [send_kv(xc, None, ep_xp), send_kv(xc, None, ep_xm)]
-    kv_mate = [send_kv(xc, None, ep_mate)]
     z_up, z_down = zs[1] * NXC + xc, zs[NZ - 1] * NXC + xc
-    q_up = [send(qg.at[z], qg.at[z], z_up, y)]
-    q_down = [send(qg.at[z], qg.at[z], z_down, y)]
+    kv_first, kv_mate, q_up, q_down = [], [], [], []
 
     def q_forward(step):
         q_up[step - 1].wait_recv()
@@ -293,6 +359,7 @@
         whole_wait(srecv.at[pl.ds(0, NZ - 1)], st_pair[1])
         waits.append(functools.partial(whole_wait, osend, o_pair[0]))
         waits.append(functools.partial(whole_wait, ssend, st_pair[0]))
+        loads[10].wait()
         rows = []
         for h in range(2):
             levels = [srecv[k, h : h + 1] for k in range(NZ)]
@@ -307,7 +374,7 @@
         attended = jnp.concatenate(rows, axis=0).T.astype(BF16)
         for c in range(CH):
             pmx[:, :, :, c * CW : (c + 1) * CW] = (
-                mm(attended, wo_ref[:, c * CW : (c + 1) * CW]).astype(BF16).reshape(NY, 2, 32, CW)
+                mm(attended, wo_v[:, c * CW : (c + 1) * CW]).astype(BF16).reshape(NY, 2, 32, CW)
             )
         return reduce_start(pmx, mxa)
 
@@ -397,72 +464,45 @@
                 mm(hidden, sdown_v[:, c * CW : (c + 1) * CW]).astype(BF16).reshape(NY, 2, 32, CW)
             )
 
-    to_expert(0)
-    kv_forward()
-    spread(0)
-    q_forward(1)
-    to_expert(1)
-    kv_last()
-    tok_second = gather_forward(tok_first, tokg)
-    spread(1)
-    spread_on(0)
-    q_forward(2)
-    to_expert(2)
-    kv_finish()
-    attend(0)
-    spread(2)
-    spread_on(1)
-    q_forward(3)
-    to_expert(3)
-    attend(1)
-    spread(3)
-    lift(0)
-    spread_on(2)
-    q_forward(4)
-    attend(7)
-    lift(1)
-    spread_on(3)
-    gather_finish(tok_second)
-    shared()
-    sh_first = reduce_start(psh, sha)
-    attend(2)
-    attend(6)
-    lift(2)
-    lift(3)
-    activate()
-    lower(0)
-    lower(1)
-    lower(2)
-    lower(3)
-    lower_on(0)
-    attend(3)
-    lower_on(1)
-    sh_second = reduce_forward(sh_first, psh, sha, shb)
-    back_x(0)
-    lower_on(2)
-    attend(5)
-    back_z(0)
-    back_x(1)
-    lower_on(3)
-    attend(4)
-    ssum[...] = reduce_finish(sh_second, psh, shb)
-    back_z(1)
-    back_x(2)
-    mx_first = project()
-    back_z(2)
-    back_x(3)
-    combine(0)
-    mx_second = reduce_forward(mx_first, pmx, mxa, mxb)
-    back_z(3)
-    combine(1)
-    combine(2)
-    mix_ref[...] = reduce_finish(mx_second, pmx, mxb).reshape(ROWS, D).astype(BF16)
-    combine(3)
+    def shared_start():
+        gather_finish(held["tok"])
+        shared()
+        held["sh"] = reduce_start(psh, sha)
+
+    def shared_on():
+        held["sh"] = reduce_forward(held["sh"], psh, sha, shb)
+
+    def shared_end():
+        ssum[...] = reduce_finish(held["sh"], psh, shb)
+
+    def tok_on():
+        held["tok"] = gather_forward(tok_first, tokg)
+
+    def mixer():
+        held["mx"] = project()
+
+    def mixer_on():
+        held["mx"] = reduce_forward(held["mx"], pmx, mxa, mxb)
+
+    def mixer_end():
+        mix_ref[...] = reduce_finish(held["mx"], pmx, mxb).reshape(ROWS, D).astype(BF16)
+
+    events = dict(
+        X=to_expert, Y=spread, F=spread_on, L=lift, A=attend, Q=q_forward, K=kv_forward,
+        K2=kv_last, K3=kv_finish, T=tok_on, S=shared_start, S2=shared_on, S3=shared_end,
+        V=activate, W=lower, W2=lower_on, B=back_x, Z=back_z, C=combine,
+        M=mixer, M2=mixer_on, M3=mixer_end, G=lat_on, P=queries_keys,
+    )
+    for item in ORDER.split():
+        name, at = (item.split(".") + [None])[:2]
+        with jax.named_scope(name if at is None else name + "_" + at):
+            events[name](*([] if at is None else [int(at)]))
+    assert used[0] <= N_SEMS
     for wait in waits:
         wait()
 
 
-N_SEMS = 160
+N_SEMS = 200
 
 
 def fused(*args):
@@ -473,11 +513,12 @@
     return pl.pallas_call(
         kernel,
         out_shape=[jax.ShapeDtypeStruct((ROWS, D), BF16)] * 2,
-        in_specs=[vmem] * 12 + [hbm] * 6,
+        in_specs=[vmem] * 10 + [hbm] * 11,
         out_specs=[vmem] * 2,
         scratch_shapes=[
             s(2, D, 256), s(2, D, 256), s(2, 256, D), s(D, 256), s(D, 256), s(256, D),
-            pltpu.SemaphoreType.DMA((6,)),
+            s(512, 128), s(512, 256), s(256, 128), s(256, 128), s(128, D), f(2, GROUP, 128),
+            pltpu.SemaphoreType.DMA((11,)),
             s(NY, 2, 32, LAT), s(NY, 2, 32, D),
             s(CH, NZ, 32, CW), s(CH, NZ, 32, CW), s(CH, NXC, 32, CW),
             s(CH, NY, 2, 4, 32, CW),
@@ -498,21 +539,12 @@
     )(*args)
 
 
-def rms_rows(entries, gain_row):
-    widened = entries.astype(F32)
-    return widened * lax.rsqrt(jnp.mean(widened * widened, -1, keepdims=True) + norm_eps) * gain_row
-
-
-def apart(columns, width, at):
-    depth = columns.shape[0]
-    blocks = columns.reshape(depth, 2, width)
-    return jnp.pad(blocks, ((0, 0), (0, 0), (at, 128 - at - width))).reshape(depth, 256)
-
-
-def halves(columns):
-    blocks = columns.reshape(columns.shape[0], -1, ROTARY // 2, 2)
-    even, odd = blocks[..., 0], blocks[..., 1]
-    return jnp.concatenate([even, odd], -1), jnp.concatenate([odd, even], -1)
+def turn_table():
+    frequency = rope_base ** (-np.arange(ROTARY // 2, dtype=np.float64) * 2.0 / ROTARY)
+    table = np.zeros((2, 128), np.float32)
+    table[0, CONTENT : CONTENT + ROTARY] = np.tile(frequency, 2)
+    table[1, CONTENT : CONTENT + ROTARY] = np.repeat([-1.0, 1.0], ROTARY // 2)
+    return jnp.asarray(table)
 
 
 def shards(
@@ -520,34 +552,10 @@
     key_content, value_weight, output_weight, expert_input, norm_gain, routes, route_weight,
     expert_gate, expert_up, expert_down, shared_gate, shared_up, shared_down,
 ):
-    y = lax.axis_index("tp")
-    start = lax.axis_index("ep") * GROUP
-    qn = rms_rows(query_latent, query_gain).astype(BF16)
-    ln = rms_rows(key_latent, latent_gain).astype(BF16)
-    en = rms_rows(expert_input, norm_gain).astype(BF16)
-    frequency = rope_base ** (-jnp.arange(ROTARY // 2, dtype=F32) * 2.0 / ROTARY)
-    angles = (start + jnp.arange(GROUP, dtype=jnp.int32)).astype(F32)[:, None] * frequency[None, :]
-    cosine, sine = jnp.cos(angles), jnp.sin(angles)
-    cos2 = jnp.concatenate([cosine, cosine], -1)
-    sin2 = jnp.concatenate([-sine, sine], -1)
-    own_cos = lax.dynamic_slice_in_dim(cos2, y * ROWS, ROWS, 0)
-    own_sin = lax.dynamic_slice_in_dim(sin2, y * ROWS, ROWS, 0)
-    straight, crossed = halves(rotary_key.astype(F32))
-    kt = (straight[:, 0] * own_cos + crossed[:, 0] * own_sin).astype(BF16)
-    kt = jnp.pad(kt, ((0, 0), (CONTENT, 128 - CONTENT - ROTARY)))
-    lat = jnp.concatenate([qn, ln, kt], -1).reshape(2, 32, LAT)
-    spread = lambda t: jnp.pad(t, ((0, 0), (CONTENT, 128 - CONTENT - ROTARY)))
-    cos_wide = jnp.tile(spread(cos2), (1, 2))
-    sin_wide = jnp.tile(spread(sin2), (1, 2))
-    cut = lambda w, width: lax.dynamic_slice_in_dim(w, y * 2 * width, 2 * width, 1)
-    wq = apart(cut(query_content, CONTENT), CONTENT, 0)
-    wr, ws = halves(cut(query_rotary, ROTARY))
-    wr, ws = apart(wr, ROTARY, CONTENT), apart(ws, ROTARY, CONTENT)
-    wk = apart(cut(key_content, CONTENT), CONTENT, 0)
-    wv = cut(value_weight, VALUE).T
     mix, out = fused(
-        lat, en.reshape(2, 32, D), routes.T, route_weight.T, cos_wide, sin_wide,
-        wq, wr, ws, wk, wv, output_weight,
+        query_latent, key_latent, rotary_key.T, query_gain[None], latent_gain[None],
+        expert_input, norm_gain[None], routes.T, route_weight.T, turn_table(),
+        query_content, query_rotary, key_content, value_weight, output_weight,
         expert_gate, expert_up, expert_down, shared_gate, shared_up, shared_down,
     )
     return mix, out

time: 157 us -> 128 us (0.82)
  Pallas kernels: 136 us -> 123 us
  local copies, waits for them, and re-layouts: 12.7 us -> 3.34 us
  other arithmetic: 6.63 us -> 0 us
    pallas_call x1, Pallas kernels: 136 us -> 123 us  [fused(): pl.pallas_call(kernel, out_shape=[jax.ShapeDtypeStruct((ROWS, D), BF16)]...]
    reshape x5 -> x0, local copies, waits for them, and re-layouts: 3.31 us -> none  [the longest x4 3.27 us: apart(): jnp.pad(blocks, ((0, 0), (0, 0), (at, 128 - at - width)))]
    reduce_sum x3 -> x0, other arithmetic: 3 us -> none  [rms_rows(): jnp.mean(widened * widened, -1, keepdims=True) + norm_eps]
    unnamed x17 -> x2, local copies, waits for them, and re-layouts: 6.03 us -> 3.34 us
    convert_element_type x5 -> x0, other arithmetic: 2.68 us -> none  [the longest x1 0.92 us: shards(): qn = rms_rows(query_latent, query_gain).astype(BF16)]
    dynamic_slice x4 -> x0, local copies, waits for them, and re-layouts: 2.02 us -> none  [shards(): lax.dynamic_slice_in_dim(w, y * 2 * width, 2 * width, 1)]
where the time goes in v2:
time: 128 us; the launch traced here: 127 us
  Pallas kernels  123 us (96%)
  local copies, waits for them, and re-layouts  3.34 us (3%)
    pallas_call x1, Pallas kernels, fused(): pl.pallas_call(kernel, out_shape=[jax.ShapeDtypeStruct((ROWS, D), BF16)]...  123 us
    unnamed x2, local copies, waits for them, and re-layouts  3.34 us

profile of v2, /device:TPU:1, one launch (start us, length us, event | category | flops | bytes accessed | tf_op | source)
XLA Modules:
  0.0 127.5 jit_solution(11415579124953827998)
XLA Ops:
  0.6 123.5 %fused.1 = (bf16[64,2048]{1,0:T(8,128)(2,1)}, bf16[64,2048]{1,0:T(8,128)(2,1)}) custom-call(bf16[64,512]{1,0:T(8,128)(2,1)} %ql_ref.1, bf16[64,256]{1,0:T(8,128)(2,1)} %kl_ref.1, bf16[32,64]{1,0:T(8,128)(2,1)} %bitcast.6, f32[1,512]{1,0:T(1,128)} %bitcast.8, f32[1,256]{1,0:T(1,128)} %bitcast.9, bf16[64,2048]{1,0:T(8,128)(2,1)} %tok_ref.1, ...), custom_call_target="tpu_custom_call" | custom-call | tf_op jit(solution)/shard_map/fused/pallas_call | solution.py:513
  124.1 1.7 %copy.25 = bf16[64,2048]{1,0:T(8,128)(2,1)} copy(bf16[64,2048]{1,0:T(8,128)(2,1)} %get-tuple-element.4) | data formatting | bytes 524288
  125.8 1.7 %copy.26 = bf16[64,2048]{1,0:T(8,128)(2,1)} copy(bf16[64,2048]{1,0:T(8,128)(2,1)} %get-tuple-element.5) | data formatting | bytes 524288

commit v3 on v2

--- a/solution.py
+++ b/solution.py
@@ -29,13 +29,19 @@
 rope_base = 10000.0
 EXP_SCALE = (CONTENT + ROTARY) ** (-0.5) * math.log2(math.e)
 
-ORDER = " ".join([
-    "X.0 G X.1 Y.0 P X.2 Y.1 X.3 F.0 Y.2 X.4 F.1 Y.3 K X.5 F.2 Y.4 X.6 F.3 Y.5 K2 X.7 F.4 Y.6 T Y.7 F.5 K3",
-    "A.0 F.6 S L.0 L.1 Q.1 A.1 F.7 S2 L.2 L.3 L.4 L.5 L.6 L.7 V",
-    "W.0 W.1 W.2 A.7 W2.0 W.3 Q.2 A.2 W2.1 W.4 A.6 W2.2 B.0 W.5 Q.3 A.3 W2.3 B.1 Z.0 W.6 A.5",
-    "W2.4 B.2 Z.1 W.7 Q.4 A.4 S3 W2.5 B.3 Z.2 C.0 W2.6 B.4 Z.3 C.1 W2.7 M B.5 Z.4 C.2 B.6 Z.5 C.3 B.7 Z.6 M2",
-    "C.4 C.5 Z.7 C.6 M3 C.7",
-])
+ORDER = (
+    ("G",), ("D",), ("X", 0), ("X", 1), ("P",), ("Y", 0), ("X", 2), ("Y", 1), ("X", 3), ("F", 0),
+    ("Y", 2), ("X", 4), ("F", 1), ("Y", 3), ("K",), ("X", 5), ("F", 2), ("Y", 4), ("X", 6), ("F", 3),
+    ("Y", 5), ("K2",), ("O",), ("X", 7), ("F", 4), ("Y", 6), ("T",), ("Y", 7), ("F", 5), ("O2",),
+    ("K3",), ("A", 0), ("F", 6), ("L", 0), ("L", 1), ("Q", 1), ("A", 1), ("F", 7), ("S",), ("L", 2),
+    ("L", 3), ("L", 4), ("L", 5), ("L", 6), ("O3",), ("L", 7), ("V",), ("W", 0), ("W", 1), ("W", 2),
+    ("A", 7), ("W2", 0), ("W", 3), ("Q", 2), ("A", 2), ("W2", 1), ("W", 4), ("A", 6), ("W2", 2),
+    ("B", 0), ("W", 5), ("Q", 3), ("A", 3), ("W2", 3), ("B", 1), ("Z", 0), ("W", 6), ("O4",), ("A", 5),
+    ("W2", 4), ("B", 2), ("Z", 1), ("W", 7), ("Q", 4), ("A", 4), ("W2", 5), ("B", 3), ("Z", 2),
+    ("W2", 6), ("B", 4), ("Z", 3), ("W2", 7), ("S2",), ("B", 5), ("Z", 4), ("B", 6), ("B", 7), ("Z", 5),
+    ("Z", 6), ("M",), ("Z", 7), ("S3",), ("C", 0), ("C", 1), ("C", 2), ("C", 3), ("C", 4), ("O5",),
+    ("M2",), ("C", 5), ("C", 6), ("C", 7),
+)
 
 
 def mm(a, b):
@@ -50,11 +56,11 @@
     ql_ref, kl_ref, rk_ref, qgain_ref, lgain_ref, tok_ref, ngain_ref, routes_ref, rw_ref, turn_ref,
     qc_hbm, qr_hbm, kc_hbm, vw_hbm, wo_hbm,
     gate_hbm, up_hbm, down_hbm, sgate_hbm, sup_hbm, sdown_hbm,
-    mix_ref, exp_ref,
-    gate_v, up_v, down_v, sgate_v, sup_v, sdown_v, qc_v, qr_v, kc_v, vw_v, wo_v, angle, wsem,
+    out_ref,
+    gate_v, up_v, down_v, sgate_v, sup_v, sdown_v, qc_v, qr_v, kc_v, vw_v, wog, angle, wsem,
     latg, tokg, s1, r1, s2, g, acc, hid, part, rsa, rsb, s3, r3, s4, r4,
     qg, kg, vg, st, osend, ssend, orecv, srecv,
-    psh, sha, shb, ssum, pmx, mxa, mxb,
+    psh, sha, shb, ssum, ats, atg,
     send_sem, recv_sem,
 ):
     ep = lax.axis_index("ep")
@@ -70,13 +76,15 @@
     zs = [lax.rem(z + d, NZ) for d in range(NZ)]
     xcs = [lax.rem(xc + d, NXC) for d in range(NXC)]
 
-    used = [0]
+    mix_ref, exp_ref = out_ref.at[0], out_ref.at[1]
+    used = [0, 0]
     waits = []
     held = {}
 
-    def sems():
-        used[0] += 1
-        return send_sem.at[used[0] - 1], recv_sem.at[used[0] - 1]
+    def sems(fresh=True):
+        used[0] += fresh
+        used[1] += 1
+        return send_sem.at[used[0] - 1], recv_sem.at[used[1] - 1]
 
     def remote(src, dst, pair, e, t):
         return pltpu.make_async_remote_copy(
@@ -90,6 +98,17 @@
         waits.append(copy.wait_send)
         return copy
 
+    def send_both(one, other, both):
+        copies, pair = [], None
+        for src, dst, e, t in (one, other):
+            mine = sems(fresh=pair is None)
+            pair = mine if pair is None else pair
+            copy = remote(src, dst, (pair[0], mine[1]), e, t)
+            copy.start()
+            copies.append(copy)
+        waits.append(functools.partial(whole_wait, both, pair[0]))
+        return copies
+
     def whole_wait(ref, sem):
         pltpu.make_async_copy(ref, ref, sem).wait()
 
@@ -98,23 +117,25 @@
         pl.semaphore_signal(barrier, inc=1, device_id=(zs[d] * NXC + xc, y), device_id_type=MESH)
     for d in range(1, NXC):
         pl.semaphore_signal(barrier, inc=1, device_id=(z * NXC + xcs[d], y), device_id_type=MESH)
-    for t in (yp, ym):
+    for t in (yp, ym, ya):
         pl.semaphore_signal(barrier, inc=1, device_id=(ep, t), device_id_type=MESH)
 
     cols = pl.ds(pl.multiple_of(y * 128, 128), 128)
+    piece = pl.ds(pl.multiple_of(xc * 256, 256), 256)
     loads = []
     for k, (src, dst) in enumerate([
         (gate_hbm, gate_v), (up_hbm, up_v), (down_hbm, down_v),
         (sgate_hbm, sgate_v), (sup_hbm, sup_v), (sdown_hbm, sdown_v),
         (qc_hbm.at[:, cols], qc_v), (qr_hbm, qr_v), (kc_hbm.at[:, cols], kc_v),
-        (vw_hbm.at[:, cols], vw_v), (wo_hbm, wo_v),
+        (vw_hbm.at[:, cols], vw_v),
+        (wo_hbm.at[0:64, piece], wog.at[xc, y, 0]), (wo_hbm.at[64:128, piece], wog.at[xc, y, 1]),
     ]):
         loads.append(pltpu.make_async_copy(src, dst, wsem.at[k]))
-    for k in (6, 7, 8, 9, 0, 1, 3, 4, 5, 2, 10):
+    for k in (10, 11, 6, 7, 8, 9, 0, 1, 3, 4, 5, 2):
         loads[k].start()
 
     def gather_start(src, buf):
-        return [send(src, buf.at[y], ep, yp), send(src, buf.at[y], ep, ym)]
+        return send_both((src, buf.at[y], ep, yp), (src, buf.at[y], ep, ym), buf.at[pl.ds(0, 2)])
 
     def gather_forward(first, buf):
         first[0].wait_recv()
@@ -128,10 +149,9 @@
         second[1].wait_recv()
 
     def reduce_start(parts, far):
-        return [
-            send(parts.at[ya, 0], far.at[0], ep, yp),
-            send(parts.at[ya, 1], far.at[1], ep, ym),
-        ]
+        return send_both(
+            (parts.at[ya, 0], far.at[0], ep, yp), (parts.at[ya, 1], far.at[1], ep, ym), parts.at[0]
+        )
 
     def reduce_forward(first, parts, far, near):
         first[0].wait_recv()
@@ -187,9 +207,12 @@
     ]
     share = [as_column(rw_ref[k : k + 1, :]) for k in range(2)]
 
-    for c in range(CH):
+    s1[0] = mm(picker, normed_rows[:, :CW]).astype(BF16).reshape(NZ, 32, CW)
+    pl.semaphore_wait(barrier, NZ - 1 + NXC - 1 + NY - 1)
+    z_wait = [exchange_z(0, s1, r1)]
+    for c in range(1, CH):
         s1[c] = mm(picker, normed_rows[:, c * CW : (c + 1) * CW]).astype(BF16).reshape(NZ, 32, CW)
-
+        z_wait.append(exchange_z(c, s1, r1))
     latg[y, :, :, :512] = normed(ql_ref, qgain_ref).reshape(2, 32, 512)
     latg[y, :, :, 512:768] = normed(kl_ref, lgain_ref).reshape(2, 32, 256)
     position = ep * GROUP + lax.broadcasted_iota(jnp.int32, (GROUP, 128), 0)
@@ -222,10 +245,10 @@
     own = pl.ds(pl.multiple_of(y * ROWS, ROWS), ROWS)
     latg[y, :, :, 768:] = (pair[0] * angle[0, own, :] + pair[1] * angle[1, own, :]).astype(BF16).reshape(2, 32, 128)
 
-    pl.semaphore_wait(barrier, NZ - 1 + NXC - 1 + 2)
     lat_first = gather_start(latg.at[y], latg)
-    z_wait = [exchange_z(c, s1, r1) for c in range(CH)]
-    tok_first = gather_start(tokg.at[y], tokg)
+    loads[10].wait()
+    loads[11].wait()
+    wo_first = gather_start(wog.at[xc, y], wog.at[xc])
 
     p_out = lax.broadcasted_iota(jnp.int32, (256, 256), 0)
     p_in = lax.broadcasted_iota(jnp.int32, (256, 256), 1)
@@ -359,7 +382,6 @@
         whole_wait(srecv.at[pl.ds(0, NZ - 1)], st_pair[1])
         waits.append(functools.partial(whole_wait, osend, o_pair[0]))
         waits.append(functools.partial(whole_wait, ssend, st_pair[0]))
-        loads[10].wait()
         rows = []
         for h in range(2):
             levels = [srecv[k, h : h + 1] for k in range(NZ)]
@@ -371,12 +393,47 @@
                 [orecv[k, h * 64 : (h + 1) * 64].astype(F32) * scaled[k] for k in range(NZ)],
             )
             rows.append(summed / total)
-        attended = jnp.concatenate(rows, axis=0).T.astype(BF16)
-        for c in range(CH):
-            pmx[:, :, :, c * CW : (c + 1) * CW] = (
-                mm(attended, wo_v[:, c * CW : (c + 1) * CW]).astype(BF16).reshape(NY, 2, 32, CW)
-            )
-        return reduce_start(pmx, mxa)
+        ats[...] = jnp.concatenate(rows, axis=0).T.astype(BF16).reshape(NY, ROWS, 128)
+        held["at"] = [send(ats.at[t], atg.at[y], ep, t) for t in (yp, ym, ya)]
+        atg[y] = ats[y]
+
+    def mix():
+        for copy in held["at"]:
+            copy.wait_recv()
+        for c in range(NXC):
+            out = jnp.zeros((ROWS, 256), F32)
+            for k in range(NY):
+                out = out + mm(atg[k], wog[c, k].reshape(128, 256)).astype(BF16).astype(F32)
+            mix_ref[:, c * 256 : (c + 1) * 256] = out.astype(BF16)
+
+    def out_on():
+        held["wo"] = gather_forward(wo_first, wog.at[xc])
+
+    def out_across():
+        gather_finish(held["wo"])
+        whole = lambda at, e: send(wog.at[at], wog.at[at], e, y)
+        held["wx"] = [whole(xc, ep_xp), whole(xc, ep_xm)]
+        held["wm"] = [whole(xc, ep_mate)]
+
+    def out_across_on():
+        first, mate_copies = held["wx"], held["wm"]
+        low, high = pl.ds(0, 2), pl.ds(2, 2)
+        first[0].wait_recv()
+        a = send(wog.at[xcm, low], wog.at[xcm, low], ep_xp, y)
+        mate_copies.append(send(wog.at[xcm], wog.at[xcm], ep_mate, y))
+        first[1].wait_recv()
+        b = send(wog.at[xcp, high], wog.at[xcp, high], ep_xm, y)
+        mate_copies.append(send(wog.at[xcp], wog.at[xcp], ep_mate, y))
+        held["wx"] = [a, b]
+
+    def out_across_last():
+        for copy in held["wx"]:
+            copy.wait_recv()
+        held["wm"].append(send(wog.at[xca], wog.at[xca], ep_mate, y))
+
+    def out_here():
+        for copy in held["wm"]:
+            copy.wait_recv()
 
     xc_pairs = {}
 
@@ -394,9 +451,7 @@
 
     def spread(c):
         whole_wait(s2.at[c, pl.ds(0, NXC - 1)], xc_pairs[c][1])
-        g_first[c] = [
-            send(g.at[c, y], g.at[c, y], ep, yp), send(g.at[c, y], g.at[c, y], ep, ym)
-        ]
+        g_first[c] = gather_start(g.at[c, y], g.at[c])
 
     def spread_on(c):
         g_second[c] = gather_forward(g_first[c], g.at[c])
@@ -476,33 +531,26 @@
         ssum[...] = reduce_finish(held["sh"], psh, shb)
 
     def tok_on():
-        held["tok"] = gather_forward(tok_first, tokg)
-
-    def mixer():
-        held["mx"] = project()
-
-    def mixer_on():
-        held["mx"] = reduce_forward(held["mx"], pmx, mxa, mxb)
-
-    def mixer_end():
-        mix_ref[...] = reduce_finish(held["mx"], pmx, mxb).reshape(ROWS, D).astype(BF16)
+        held["tok"] = gather_forward(held["tok"], tokg)
+
+    def tok_start():
+        held["tok"] = gather_start(tokg.at[y], tokg)
 
     events = dict(
         X=to_expert, Y=spread, F=spread_on, L=lift, A=attend, Q=q_forward, K=kv_forward,
         K2=kv_last, K3=kv_finish, T=tok_on, S=shared_start, S2=shared_on, S3=shared_end,
         V=activate, W=lower, W2=lower_on, B=back_x, Z=back_z, C=combine,
-        M=mixer, M2=mixer_on, M3=mixer_end, G=lat_on, P=queries_keys,
+        M=project, M2=mix, O=out_on, O2=out_across, O3=out_across_on, O4=out_across_last, O5=out_here, G=lat_on, D=tok_start, P=queries_keys,
     )
-    for item in ORDER.split():
-        name, at = (item.split(".") + [None])[:2]
-        with jax.named_scope(name if at is None else name + "_" + at):
-            events[name](*([] if at is None else [int(at)]))
-    assert used[0] <= N_SEMS
+    for item in ORDER:
+        with jax.named_scope("_".join(map(str, item))):
+            events[item[0]](*item[1:])
+    assert used == [N_SEND, N_RECV], used
     for wait in waits:
         wait()
 
 
-N_SEMS = 200
+N_SEND, N_RECV = 128, 148
 
 
 def fused(*args):
@@ -512,13 +560,13 @@
     f = lambda *shape: pltpu.VMEM(shape, F32)
     return pl.pallas_call(
         kernel,
-        out_shape=[jax.ShapeDtypeStruct((ROWS, D), BF16)] * 2,
+        out_shape=jax.ShapeDtypeStruct((2, ROWS, D), BF16),
         in_specs=[vmem] * 10 + [hbm] * 11,
-        out_specs=[vmem] * 2,
+        out_specs=vmem,
         scratch_shapes=[
             s(2, D, 256), s(2, D, 256), s(2, 256, D), s(D, 256), s(D, 256), s(256, D),
-            s(512, 128), s(512, 256), s(256, 128), s(256, 128), s(128, D), f(2, GROUP, 128),
-            pltpu.SemaphoreType.DMA((11,)),
+            s(512, 128), s(512, 256), s(256, 128), s(256, 128), s(NXC, NY, 2, 64, 256), f(2, GROUP, 128),
+            pltpu.SemaphoreType.DMA((12,)),
             s(NY, 2, 32, LAT), s(NY, 2, 32, D),
             s(CH, NZ, 32, CW), s(CH, NZ, 32, CW), s(CH, NXC, 32, CW),
             s(CH, NY, 2, 4, 32, CW),
@@ -529,8 +577,8 @@
             f(2, NXC, GROUP, GROUP),
             s(NZ - 1, 128, GROUP), f(NZ - 1, 8, GROUP), s(NZ, 128, GROUP), f(NZ, 8, GROUP),
             s(NY, 2, 32, D), s(2, 32, D), s(2, 2, 32, D), f(2, 32, D),
-            s(NY, 2, 32, D), s(2, 32, D), s(2, 2, 32, D),
-            pltpu.SemaphoreType.DMA((N_SEMS,)), pltpu.SemaphoreType.DMA((N_SEMS,)),
+            s(NY, ROWS, 128), s(NY, ROWS, 128),
+            pltpu.SemaphoreType.DMA((N_SEND,)), pltpu.SemaphoreType.DMA((N_RECV,)),
         ],
         compiler_params=pltpu.CompilerParams(
             collective_id=0, has_side_effects=True, vmem_limit_bytes=60 * 1024 * 1024
@@ -552,13 +600,13 @@
     key_content, value_weight, output_weight, expert_input, norm_gain, routes, route_weight,
     expert_gate, expert_up, expert_down, shared_gate, shared_up, shared_down,
 ):
-    mix, out = fused(
+    both = fused(
         query_latent, key_latent, rotary_key.T, query_gain[None], latent_gain[None],
         expert_input, norm_gain[None], routes.T, route_weight.T, turn_table(),
         query_content, query_rotary, key_content, value_weight, output_weight,
         expert_gate, expert_up, expert_down, shared_gate, shared_up, shared_down,
     )
-    return mix, out
+    return both[0].astype(BF16), both[1].astype(BF16)
 
 
 def solution(mesh):

time: 128 us -> 118 us (0.922)
  Pallas kernels: 123 us -> 115 us
  local copies, waits for them, and re-layouts: 3.34 us -> 1.87 us
    pallas_call x1, Pallas kernels: 123 us -> 115 us  [fused(): pl.pallas_call(kernel, out_shape=jax.ShapeDtypeStruct((2, ROWS, D), BF16)...]
    unnamed x2 -> x0, local copies, waits for them, and re-layouts: 3.34 us -> none
    squeeze x0 -> x1, local copies, waits for them, and re-layouts: none -> 1.87 us  [shards(): return (both[0].astype(BF16), both[1].astype(BF16))]
where the time goes in v3:
time: 118 us; the launch traced here: 117 us
  Pallas kernels  115 us (97%)
  local copies, waits for them, and re-layouts  1.87 us (2%)
    pallas_call x1, Pallas kernels, fused(): pl.pallas_call(kernel, out_shape=jax.ShapeDtypeStruct((2, ROWS, D), BF16)...  115 us

profile of v3, /device:TPU:1, one launch (start us, length us, event | category | flops | bytes accessed | tf_op | source)
XLA Modules:
  0.0 117.4 jit_solution(10061475483301138300)
XLA Ops:
  0.6 114.9 %fused.1 = bf16[2,64,2048]{2,1,0:T(8,128)(2,1)} custom-call(bf16[64,512]{1,0:T(8,128)(2,1)} %ql_ref.1, bf16[64,256]{1,0:T(8,128)(2,1)} %kl_ref.1, bf16[32,64]{1,0:T(8,128)(2,1)} %bitcast.10, f32[1,512]{1,0:T(1,128)} %bitcast.12, f32[1,256]{1,0:T(1,128)} %bitcast.13, bf16[64,2048]{1,0:T(8,128)(2,1)} %tok_ref.1, f32[1,2048]{1,0:T(1,128)} %bitcast.11, ...), custom_call_target="tpu_custom_call" | custom-call | tf_op jit(solution)/shard_map/fused/pallas_call | solution.py:561
  115.5 1.9 %slice_bitcast_fusion = (bf16[64,2048]{1,0:T(8,128)(2,1)}, bf16[64,2048]{1,0:T(8,128)(2,1)}) fusion(bf16[2,64,2048]{2,1,0:T(8,128)(2,1)} %fused.1), kind=kLoop, calls=%fused_computation | loop fusion | bytes 1048576 | tf_op jit(solution)/shard_map/squeeze | solution.py:609
